TPU v7x, 256 devices: a whole 4x4x8 slice. The times are simulated.
256 devices in a mesh: sp: 32 (over z, y), tp: 8 (over x, core).
Axes of the slice: x: 4, y: 4, z: 8, core: 2. Of those that a mesh axis runs over, the one named last changes fastest.
Arguments:
- tokens: bfloat16 [32768, 2048], P('sp'), may hold values from -6 to 6
- in_gain: float32 [2048], replicated, may hold values from 0.1 to 1.9
- w_query: bfloat16 [2048, 1024], P(None, 'tp'), may hold values from -0.125 to 0.125
- w_forget: bfloat16 [2048, 1024], P(None, 'tp'), may hold values from -0.125 to 0.125
- w_input: bfloat16 [2048, 1024], P(None, 'tp'), may hold values from -0.125 to 0.125
- w_outgate: bfloat16 [2048, 1024], P(None, 'tp'), may hold values from -0.125 to 0.125
- w_conv_h: bfloat16 [2048, 1024], P(None, 'tp'), may hold values from -0.125 to 0.125
- w_conv_b: bfloat16 [2048, 1024], P(None, 'tp'), may hold values from -0.125 to 0.125
- w_conv_c: bfloat16 [2048, 1024], P(None, 'tp'), may hold values from -0.125 to 0.125
- forget_floor: float32 [1024], P('tp'), may hold values from 0.84 to 1
- forget_leak: float32 [32768, 1024], P('sp', 'tp'), may hold values from -1 to 0
- state_gain: float32 [128], replicated, may hold values from 0.1 to 1.9
- conv_taps: bfloat16 [3, 1024], P(None, 'tp'), may hold values from -3.5 to 3.5
- group_gain: float32 [128], replicated, may hold values from 0.1 to 1.9
- out_state: bfloat16 [1024, 2048], P('tp'), may hold values from -0.1875 to 0.1875
- out_conv: bfloat16 [1024, 2048], P('tp'), may hold values from -0.1875 to 0.1875
Outputs:
- mixed_out: bfloat16 [32768, 2048], P('sp', 'tp')
All inputs are finite; a program needn't handle non-finite values.
Results may differ from a plain program's by a relative error of at most 0.015.
Values may be sent and summed in bfloat16 or wider, within the bound.
A program may use at most 128 MiB of HBM per device.

v0:
```python
import functools

import jax
import jax.numpy as jnp
from jax import lax
from jax.experimental import pallas as pl
from jax.experimental.pallas import tpu as pltpu
from jax.sharding import PartitionSpec as P

GROUP_FEATURES = 128
CHUNK = 128
ROWS = 256
TAPS = 3
HALO = 8

norm_eps = 1e-06
f32 = jnp.float32
bf16 = jnp.bfloat16


def dot(a, b, dims=((1,), (0,)), precision=None):
    return lax.dot_general(a, b, (dims, ((), ())), precision=precision, preferred_element_type=f32)


def rms(values):
    return values * lax.rsqrt(jnp.mean(values * values, axis=-1, keepdims=True) + norm_eps)


def per_group(values, gain):
    parts = []
    for g in range(values.shape[1] // GROUP_FEATURES):
        parts.append(rms(values[:, g * GROUP_FEATURES : (g + 1) * GROUP_FEATURES]) * gain)
    return jnp.concatenate(parts, axis=1)


def fused_kernel(
    tp, sp,
    tokens, in_gain, wq, wf, wi, wg, wh, wb, wc, floor, leak, state_gain, taps, group_gain,
    out_state, out_conv, result,
    pad, state, offset, read, qdev, gate, conv_all, mix_all, columns, states, logs, sent_state,
    rim, tail, head_conv, head_gate, incoming,
    col_send, col_recv, own_sem, blk_send, fwd_send, blk_recv, st_send, st_recv, log_send, log_recv,
    rim_send, rim_recv,
):
    step, steps = pl.program_id(0), pl.num_programs(0)
    rows = tokens.shape[0]
    me, place = lax.axis_index("tp"), lax.axis_index("sp")
    partner = me + 1 - 2 * lax.rem(me, 2)
    ncols = result.shape[1]
    heads = state.shape[0]
    here = pl.ds(pl.multiple_of(step * rows, rows), rows)
    held = (conv_all, mix_all)

    def col_copy(kind, k):
        target = lax.rem(me + k, tp)
        src = (out_state, out_conv)[kind].at[:, pl.ds(pl.multiple_of(target * ncols, ncols), ncols)]
        dst = columns.at[kind, me]
        if k == 0:
            return pltpu.make_async_copy(src, dst, own_sem.at[kind])
        return pltpu.make_async_remote_copy(
            src, dst, col_send.at[kind, k], col_recv.at[kind, me], device_id={"tp": target}
        )

    def block_copy(kind, t, origin, target, send):
        ref = held[kind].at[origin, t]
        return pltpu.make_async_remote_copy(
            ref, ref, send, blk_recv.at[kind, origin, t], device_id={"tp": target}
        )

    def own_copies(kind, t):
        out = [block_copy(kind, t, me, partner, blk_send.at[kind, 0, t])]
        for k in range(1, tp // 2):
            out.append(block_copy(kind, t, me, lax.rem(me + 2 * k, tp), blk_send.at[kind, k, t]))
        return out

    def relays(kind, t):
        out = []
        for k in range(1, tp // 2):
            origin = lax.rem(me + 2 * k, tp)
            out.append(block_copy(kind, t, origin, partner, fwd_send.at[kind, k, t]))
        return out

    def state_copies(k):
        target = lax.rem(place + k, sp)
        to = {"sp": target}
        return (
            pltpu.make_async_remote_copy(
                sent_state, states.at[place], st_send.at[k], st_recv.at[place], device_id=to
            ),
            pltpu.make_async_remote_copy(
                offset, logs.at[place], log_send.at[k], log_recv.at[place], device_id=to
            ),
        )

    def state_arrivals(k):
        source = lax.rem(place + k, sp)
        to = {"sp": source}
        return (
            pltpu.make_async_remote_copy(
                sent_state, states.at[source], st_send.at[k], st_recv.at[source], device_id=to
            ),
            pltpu.make_async_remote_copy(
                offset, logs.at[source], log_send.at[k], log_recv.at[source], device_id=to
            ),
        )

    rim_copy = pltpu.make_async_remote_copy(
        tail, rim, rim_send.at[0], rim_recv.at[0], device_id={"sp": lax.rem(place + 1, sp)}
    )

    @pl.when(step == 0)
    def _():
        barrier = pltpu.get_barrier_semaphore()
        for k in range(1, tp):
            pl.semaphore_signal(barrier, inc=1, device_id={"tp": lax.rem(me + k, tp)})
        for k in range(1, sp):
            pl.semaphore_signal(barrier, inc=1, device_id={"sp": lax.rem(place + k, sp)})
        pl.semaphore_wait(barrier, tp + sp - 2)
        for kind in (1, 0):
            for k in range(tp):
                col_copy(kind, k).start()
        pad[0:HALO, :] = jnp.zeros((HALO, pad.shape[1]), f32)
        state[...] = jnp.zeros_like(state)
        offset[...] = jnp.zeros_like(offset)

    normed = (rms(tokens[...].astype(f32)) * in_gain[...]).astype(bf16)

    def project(w):
        return dot(normed, w[...]).astype(bf16).astype(f32)

    conv_in = (project(wc) * project(wh)).astype(bf16).astype(f32)
    proj_b = project(wb)
    pad[HALO : HALO + rows, :] = conv_in
    w = taps[...].astype(f32)
    total = w[TAPS - 1 : TAPS] * conv_in
    for j in range(TAPS - 1):
        total += w[j : j + 1] * pad[HALO - (TAPS - 1) + j : HALO - (TAPS - 1) + j + rows, :]
    conv_all[me, step] = per_group(proj_b * total, group_gain[...]).astype(bf16)

    @pl.when(step == 0)
    def _():
        head_conv[...] = conv_in[:HALO]
        head_gate[...] = proj_b[:HALO]

    pad[0:HALO, :] = conv_in[rows - HALO :]

    x = project(wf)
    key = (1.0 - floor[...]) * jax.nn.sigmoid(-x)
    logf = jnp.log(1.0 - key) + leak[...]
    value = dot(normed, wi[...]).astype(bf16)
    query = jax.nn.silu(project(wq))
    gate[here, :] = dot(normed, wg[...]).astype(bf16)

    r = lax.broadcasted_iota(jnp.int32, (CHUNK, CHUNK), 0)
    c = lax.broadcasted_iota(jnp.int32, (CHUNK, CHUNK), 1)
    causal = r >= c
    ones = causal.astype(f32)
    for b in range(rows // CHUNK):
        lo, hi = b * CHUNK, (b + 1) * CHUNK
        at = pl.ds(pl.multiple_of(step * rows + lo, CHUNK), CHUNK)
        cum = dot(ones, logf[lo:hi], precision=lax.Precision.HIGHEST)
        mid = cum[CHUNK // 2 - 1 : CHUNK // 2]
        last = cum[CHUNK - 1 : CHUNK]
        q_mid = query[lo:hi] * jnp.exp(cum - mid)
        k_mid = key[lo:hi] * jnp.exp(mid - cum)
        q_all = q_mid * jnp.exp(mid)
        k_end = (k_mid * jnp.exp(last - mid)).astype(bf16)
        qdev[at, :] = (q_all * jnp.exp(offset[0:1, :])).astype(bf16)
        q_mid, k_mid, q_all = q_mid.astype(bf16), k_mid.astype(bf16), q_all.astype(bf16)
        for h in range(heads):
            s = slice(h * GROUP_FEATURES, (h + 1) * GROUP_FEATURES)
            scores = dot(q_mid[:, s], k_mid[:, s], ((1,), (1,)))
            scores = jnp.where(causal, scores, 0.0).astype(bf16)
            v = value[lo:hi, s]
            old = state[h]
            read[at, s] = dot(scores, v) + dot(q_all[:, s], old.astype(bf16), ((1,), (1,)))
            state[h] = old * jnp.exp(last[:, s]) + dot(v, k_end[:, s], ((0,), (0,)))
        offset[...] += last

    @pl.when(step > 0)
    def _():
        for copy in own_copies(0, step):
            copy.start()

    @pl.when(step == steps - 1)
    def _():
        nb = read.shape[0] // rows
        tail[...] = pad[0:HALO, :]
        sent_state[...] = state[...].astype(bf16)
        rim_copy.start()
        for k in range(1, sp):
            for copy in state_copies(k):
                copy.start()
        rim_copy.wait_recv()
        before = jnp.where(place > 0, rim[...], 0.0)
        ext = jnp.concatenate([before, head_conv[...]], axis=0)
        fixed = w[TAPS - 1 : TAPS] * head_conv[...]
        for j in range(TAPS - 1):
            fixed += w[j : j + 1] * ext[HALO - (TAPS - 1) + j : 2 * HALO - (TAPS - 1) + j]
        fixed = per_group(head_gate[...] * fixed, group_gain[...])
        conv_all[me, 0, 0:HALO, :] = fixed.astype(bf16)

        for k in range(1, sp):
            for copy in state_arrivals(k):
                copy.wait_recv()
        for copy in own_copies(0, 0):
            copy.start()
        incoming[...] = jnp.zeros_like(incoming)

        def hop(p, _):
            decay = jnp.exp(logs[p, 0:1, :])
            for h in range(heads):
                s = slice(h * GROUP_FEATURES, (h + 1) * GROUP_FEATURES)
                incoming[h] = incoming[h] * decay[:, s] + states[p, h].astype(f32)
            return 0

        lax.fori_loop(0, place, hop, 0)

        def merge(t, _):
            at = pl.ds(pl.multiple_of(t * rows, rows), rows)
            for h in range(heads):
                s = slice(h * GROUP_FEATURES, (h + 1) * GROUP_FEATURES)
                whole = read[at, s] + dot(qdev[at, s], incoming[h].astype(bf16), ((1,), (1,)))
                out = rms(whole) * state_gain[...] * jax.nn.silu(gate[at, s].astype(f32))
                mix_all[me, t, :, s] = out.astype(bf16)
            for copy in own_copies(1, t):
                copy.start()
            return 0

        lax.fori_loop(0, nb, merge, 0)

        def relay(kind, t):
            for copy in relays(kind, t):
                copy.wait_recv()
                copy.start()

        def conv_relay(t, _):
            relay(0, t + 1)
            return 0

        lax.fori_loop(0, nb - 1, conv_relay, 0)
        relay(0, 0)
        for kind in range(2):
            col_copy(kind, 0).wait()
            for k in range(1, tp):
                source = lax.rem(me + k, tp)
                ref = columns.at[kind, source]
                pltpu.make_async_remote_copy(
                    ref, ref, col_send.at[kind, k], col_recv.at[kind, source],
                    device_id={"tp": source},
                ).wait_recv()

        def finish(t, _):
            relay(1, t)
            for kind in range(2):
                for k in range(tp // 2):
                    origin = lax.rem(partner + 2 * k, tp)
                    block_copy(kind, t, origin, partner, blk_send.at[kind, 0, t]).wait_recv()
            acc = jnp.zeros((rows, ncols), f32)
            for o in range(tp):
                acc += dot(mix_all[o, t], columns[0, o])
                acc += dot(conv_all[o, t], columns[1, o])
            result[pl.ds(pl.multiple_of(t * rows, rows), rows), :] = acc.astype(bf16)
            return 0

        lax.fori_loop(0, nb, finish, 0)

        def drain(t, _):
            for kind in range(2):
                for copy in own_copies(kind, t) + relays(kind, t):
                    copy.wait_send()
            return 0

        lax.fori_loop(0, nb, drain, 0)
        for kind in range(2):
            for k in range(1, tp):
                col_copy(kind, k).wait_send()
        rim_copy.wait_send()
        for k in range(1, sp):
            for copy in state_copies(k):
                copy.wait_send()


def body(
    tokens, in_gain, w_query, w_forget, w_input, w_outgate, w_conv_h, w_conv_b, w_conv_c,
    forget_floor, forget_leak, state_gain, conv_taps, group_gain, out_state, out_conv,
):
    count, feats = tokens.shape
    width, channels = w_query.shape[1], w_conv_h.shape[1]
    heads = width // GROUP_FEATURES
    tp, sp = lax.axis_size("tp"), lax.axis_size("sp")
    ncols, nb = out_state.shape[1] // tp, count // ROWS

    def whole(*shape):
        return pl.BlockSpec(shape, lambda i: (0,) * len(shape))

    def rows(n):
        return pl.BlockSpec((ROWS, n), lambda i: (i, 0))

    sems = pltpu.SemaphoreType.DMA
    return pl.pallas_call(
        functools.partial(fused_kernel, tp, sp),
        grid=(nb,),
        in_specs=[rows(feats), whole(1, feats)] + [whole(feats, width)] * 4
        + [whole(feats, channels)] * 3
        + [whole(1, width), rows(width), whole(1, GROUP_FEATURES), whole(TAPS, channels),
           whole(1, GROUP_FEATURES)]
        + [pl.BlockSpec(memory_space=pl.ANY)] * 2,
        out_specs=whole(count, ncols),
        out_shape=jax.ShapeDtypeStruct((count, ncols), bf16),
        scratch_shapes=[
            pltpu.VMEM((HALO + ROWS, channels), f32),
            pltpu.VMEM((heads, GROUP_FEATURES, GROUP_FEATURES), f32),
            pltpu.VMEM((HALO, width), f32),
            pltpu.VMEM((count, width), f32),
            pltpu.VMEM((count, width), bf16),
            pltpu.VMEM((count, width), bf16),
            pltpu.VMEM((tp, nb, ROWS, channels), bf16),
            pltpu.VMEM((tp, nb, ROWS, width), bf16),
            pltpu.VMEM((2, tp, width, ncols), bf16),
            pltpu.VMEM((sp, heads, GROUP_FEATURES, GROUP_FEATURES), bf16),
            pltpu.VMEM((sp, HALO, width), f32),
            pltpu.VMEM((heads, GROUP_FEATURES, GROUP_FEATURES), bf16),
            pltpu.VMEM((HALO, channels), f32),
            pltpu.VMEM((HALO, channels), f32),
            pltpu.VMEM((HALO, channels), f32),
            pltpu.VMEM((HALO, channels), f32),
            pltpu.VMEM((heads, GROUP_FEATURES, GROUP_FEATURES), f32),
            sems((2, tp)), sems((2, tp)), sems((2,)),
            sems((2, tp // 2, nb)), sems((2, tp // 2, nb)), sems((2, tp, nb)),
            sems((sp,)), sems((sp,)), sems((sp,)), sems((sp,)), sems((1,)), sems((1,)),
        ],
        compiler_params=pltpu.CompilerParams(
            vmem_limit_bytes=56 * 2**20, collective_id=0, has_side_effects=True
        ),
    )(
        tokens, in_gain[None], w_query, w_forget, w_input, w_outgate, w_conv_h, w_conv_b, w_conv_c,
        forget_floor[None], forget_leak, state_gain[None], conv_taps, group_gain[None],
        out_state, out_conv,
    )


def solution(mesh):
    cols, rows = P(None, "tp"), P("tp", None)
    in_specs = (
        P("sp", None), P(), cols, cols, cols, cols, cols, cols, cols,
        P("tp"), P("sp", "tp"), P(), cols, P(), rows, rows,
    )
    return jax.shard_map(
        body, mesh=mesh, in_specs=in_specs, out_specs=P("sp", "tp"), check_vma=False
    )
```

profile of v0, /device:TPU:1, one launch (start us, length us, event | category | flops | bytes accessed | tf_op | source)
XLA Modules:
  0.0 77.2 jit_solution(9053022233309903120)
XLA Ops:
  0.0 75.4 %shard_map.154 = bf16[1024,256]{1,0:T(8,128)(2,1)} custom-call(bf16[1024,2048]{1,0:T(8,128)(2,1)} %tokens.1, f32[1,2048]{1,0:T(1,128)} %bitcast.4, bf16[2048,128]{1,0:T(8,128)(2,1)} %wq.1, bf16[2048,128]{1,0:T(8,128)(2,1)} %wf.1, bf16[2048,128]{1,0:T(8,128)(2,1)} %wi.1, bf16[2048,128]{1,0:T(8,128)(2,1)} %wg.1, bf16[2048,128]{1,0:T(8,128)(2,1)} %wh.1, ...), custom_call_target="tpu_custom_call" | custom-call | tf_op jit(solution)/shard_map/pallas_call | solution.py:301
  75.4 1.9 %copy.18 = bf16[1024,256]{1,0:T(8,128)(2,1)} copy(bf16[1024,256]{1,0:T(8,128)(2,1)} %shard_map.154) | data formatting | bytes 1048576
where the time goes:
time: 77.8 us; the launch traced here: 77.2 us
  Pallas kernels  75.4 us (97%)
  local copies, waits for them, and re-layouts  1.87 us (2%)
    pallas_call x1, Pallas kernels, body(): pl.pallas_call(functools.partial(fused_kernel, tp, sp), grid=(nb,), in_sp...  75.4 us
    unnamed x1, local copies, waits for them, and re-layouts  1.87 us

commit v1 on v0

v1 whole, which is shorter than its diff:
```python
import functools

import jax
import jax.numpy as jnp
from jax import lax
from jax.experimental import pallas as pl
from jax.experimental.pallas import tpu as pltpu
from jax.sharding import PartitionSpec as P

GROUP = 128
CHUNK = 128
ROWS = 256
TAPS = 3
HALO = 8
NY = 4
LOGS = 16

norm_eps = 1e-06
f32 = jnp.float32
bf16 = jnp.bfloat16


def dot(a, b, dims=((1,), (0,))):
    return lax.dot_general(a, b, (dims, ((), ())), preferred_element_type=f32)


def rms(values):
    return values * lax.rsqrt(jnp.mean(values * values, axis=-1, keepdims=True) + norm_eps)


def split3(values):
    hi = values.astype(bf16)
    rest = values - hi.astype(f32)
    mid = rest.astype(bf16)
    low = (rest - mid.astype(f32)).astype(bf16)
    return hi, mid, low


def fused_kernel(
    tp, ny, nz,
    tokens, in_gain, wq, wf, wi, wg, wh, wb, wc, floor, leak, state_gain, taps, group_gain,
    out_state, out_conv, result,
    tok, w, leakv, cols, mixed, kmid, val, emid, old, stats, gate, read, qdev,
    pad, state, offset, incoming, ybuf, zbuf, rim, tail, head_conv, head_gate,
    tok_sem, w_sem, leak_sem, own_sem,
    colx_send, colx_recv, coly_send, coly_recv,
    y_send, y_recv, z_send, z_recv, rim_send, rim_recv, blk_send, blk_recv,
):
    me, place = lax.axis_index("tp"), lax.axis_index("sp")
    sp = ny * nz
    core, chip = lax.rem(me, 2), lax.div(me, 2)
    partner = me + 1 - 2 * core
    yy, zz = lax.rem(place, ny), lax.div(place, ny)
    up, down, far = lax.rem(me + 2, tp), lax.rem(me + tp - 2, tp), lax.rem(me + 4, tp)
    ahead = lax.rem(me + tp + 2 - 4 * core, tp)
    behind = lax.rem(me + tp - 2 + 4 * core, tp)
    count, ncols = result.shape
    nb = count // ROWS
    nchunk = count // CHUNK
    part = GROUP // ny
    outs = (out_state, out_conv)

    def rows_at(t):
        return pl.ds(pl.multiple_of(t * ROWS, ROWS), ROWS)

    def tok_copy(t):
        return pltpu.make_async_copy(tokens.at[rows_at(t)], tok.at[rows_at(t)], tok_sem.at[t])

    weights = (wf, wi, wc, wh, wb, wg, wq)

    def w_copy(i):
        return pltpu.make_async_copy(weights[i], w.at[:, i * GROUP : (i + 1) * GROUP], w_sem.at[i])

    leak_copy = pltpu.make_async_copy(leak, leakv, leak_sem.at[0])

    def col_slice(target):
        return pl.ds(pl.multiple_of(target * ncols, ncols), ncols)

    mine_rows = pl.ds(pl.multiple_of(yy * part, part), part)

    def own_cols(kind):
        return pltpu.make_async_copy(
            outs[kind].at[:, col_slice(me)], cols.at[kind * tp + me], own_sem.at[kind]
        )

    def partner_cols(kind):
        return pltpu.make_async_remote_copy(
            outs[kind].at[:, col_slice(partner)], cols.at[kind * tp + me],
            colx_send.at[kind, 0], colx_recv.at[kind, me], device_id={"tp": partner},
        )

    def partner_cols_in(kind):
        return pltpu.make_async_remote_copy(
            outs[kind].at[:, col_slice(partner)], cols.at[kind * tp + partner],
            colx_send.at[kind, 0], colx_recv.at[kind, partner], device_id={"tp": partner},
        )

    def far_cols(kind, k):
        target = lax.rem(2 * chip + 2 + k, tp)
        return pltpu.make_async_remote_copy(
            outs[kind].at[mine_rows, col_slice(target)], cols.at[kind * tp + me, mine_rows],
            colx_send.at[kind, k + 1], colx_recv.at[kind, me], device_id={"tp": target},
        )

    def far_cols_in(kind, k):
        source = lax.rem(2 * chip + 2 + k, tp)
        return pltpu.make_async_remote_copy(
            outs[kind].at[mine_rows, col_slice(source)], cols.at[kind * tp + source, mine_rows],
            colx_send.at[kind, k + 1], colx_recv.at[kind, source], device_id={"tp": source},
        )

    def share_cols(kind, j, r):
        pair = pl.ds(kind * tp + lax.rem(2 * chip + 2 * j, tp), 2)
        ref = cols.at[pair, mine_rows]
        peer = lax.rem(yy + r, ny)
        return pltpu.make_async_remote_copy(
            ref, ref, coly_send.at[kind, j, r], coly_recv.at[kind, j, yy],
            device_id={"sp": zz * ny + peer},
        )

    def share_cols_in(kind, j, r):
        pair = pl.ds(kind * tp + lax.rem(2 * chip + 2 * j, tp), 2)
        peer = lax.rem(yy + r, ny)
        ref = cols.at[pair, pl.ds(pl.multiple_of(peer * part, part), part)]
        return pltpu.make_async_remote_copy(
            ref, ref, coly_send.at[kind, j, r], coly_recv.at[kind, j, peer],
            device_id={"sp": zz * ny + peer},
        )

    def y_copy(r):
        ref = ybuf.at[yy]
        return pltpu.make_async_remote_copy(
            ref, ref, y_send.at[r], y_recv.at[yy],
            device_id={"sp": zz * ny + lax.rem(yy + r, ny)},
        )

    def y_arrival(r):
        peer = lax.rem(yy + r, ny)
        ref = ybuf.at[peer]
        return pltpu.make_async_remote_copy(
            ref, ref, y_send.at[r], y_recv.at[peer], device_id={"sp": zz * ny + peer}
        )

    def z_copy(target):
        ref = zbuf.at[zz]
        return pltpu.make_async_remote_copy(
            ref, ref, z_send.at[target], z_recv.at[zz], device_id={"sp": target * ny + yy}
        )

    def z_arrival(source):
        ref = zbuf.at[source]
        return pltpu.make_async_remote_copy(
            ref, ref, z_send.at[source], z_recv.at[source], device_id={"sp": source * ny + yy}
        )

    rim_copy = pltpu.make_async_remote_copy(
        tail, rim, rim_send.at[0], rim_recv.at[0], device_id={"sp": lax.rem(place + 1, sp)}
    )

    def block_copy(kind, t, origin, target, slot):
        lanes = pl.ds(pl.multiple_of((kind * tp + origin) * GROUP, GROUP), GROUP)
        ref = mixed.at[t, :, lanes]
        return pltpu.make_async_remote_copy(
            ref, ref, blk_send.at[kind, slot, t], blk_recv.at[kind, origin, t],
            device_id={"tp": target},
        )

    def own_copies(kind, t):
        return [
            block_copy(kind, t, me, ahead, 1),
            block_copy(kind, t, me, behind, 2),
            block_copy(kind, t, me, partner, 0),
        ]

    def near_relays(kind, t):
        return [
            block_copy(kind, t, behind, ahead, 3),
            block_copy(kind, t, behind, partner, 4),
            block_copy(kind, t, ahead, partner, 5),
        ]

    def far_relay(kind, t):
        return block_copy(kind, t, far, partner, 6)

    def arrival(kind, t, origin):
        return block_copy(kind, t, origin, partner, 0)

    def relay_first(kind, t):
        first, second, third = near_relays(kind, t)
        arrival(kind, t, behind).wait_recv()
        first.start()
        second.start()
        arrival(kind, t, ahead).wait_recv()
        third.start()

    def relay_second(kind, t):
        arrival(kind, t, far).wait_recv()
        far_relay(kind, t).start()

    def put(kind, t, value):
        lanes = pl.ds(pl.multiple_of((kind * tp + me) * GROUP, GROUP), GROUP)
        mixed[t, :, lanes] = value

    for i in (0, 1):
        w_copy(i).start()
    tok_copy(0).start()
    leak_copy.start()
    for t in range(1, nb):
        tok_copy(t).start()
    for i in range(2, 7):
        w_copy(i).start()
    barrier = pltpu.get_barrier_semaphore()
    for k in range(1, tp):
        pl.semaphore_signal(barrier, inc=1, device_id={"tp": lax.rem(me + k, tp)})
    for r in range(1, ny):
        pl.semaphore_signal(barrier, inc=1, device_id={"sp": zz * ny + lax.rem(yy + r, ny)})
    for r in range(1, nz):
        pl.semaphore_signal(barrier, inc=1, device_id={"sp": lax.rem(zz + r, nz) * ny + yy})
    pl.semaphore_signal(barrier, inc=1, device_id={"sp": lax.rem(place + 1, sp)})
    pl.semaphore_signal(barrier, inc=1, device_id={"sp": lax.rem(place + sp - 1, sp)})
    pl.semaphore_wait(barrier, tp + ny + nz - 3 + 2)
    for kind in range(2):
        for k in range(tp - 2):
            far_cols(kind, k).start()
    for kind in range(2):
        partner_cols(kind).start()
        own_cols(kind).start()
    pad[0:HALO, :] = jnp.zeros((HALO, GROUP), f32)
    state[...] = jnp.zeros_like(state)
    offset[...] = jnp.zeros_like(offset)

    row = lax.broadcasted_iota(jnp.int32, (CHUNK, CHUNK), 0)
    col = lax.broadcasted_iota(jnp.int32, (CHUNK, CHUNK), 1)
    causal = row >= col
    ones = causal.astype(bf16)

    w_copy(0).wait()
    w_copy(1).wait()
    leak_copy.wait()

    def states(t, _):
        here = rows_at(t)
        tok_copy(t).wait()
        normed = (rms(tok[here, :].astype(f32)) * in_gain[...]).astype(bf16)
        tok[here, :] = normed
        both = dot(normed, w[:, 0 : 2 * GROUP])
        x = both[:, :GROUP].astype(bf16).astype(f32)
        value = both[:, GROUP:].astype(bf16)
        val[here, :] = value
        key = (1.0 - floor[...]) * jax.nn.sigmoid(-x)
        logf = jnp.log(1.0 - key) + leakv[here, :]
        for b in range(ROWS // CHUNK):
            lo, hi = b * CHUNK, (b + 1) * CHUNK
            at = pl.ds(pl.multiple_of(t * ROWS + lo, CHUNK), CHUNK)
            chunk = t * (ROWS // CHUNK) + b
            sums = dot(ones, jnp.concatenate(split3(logf[lo:hi]), axis=1))
            cum = sums[:, :GROUP] + sums[:, GROUP : 2 * GROUP] + sums[:, 2 * GROUP :]
            mid = cum[CHUNK // 2 - 1 : CHUNK // 2]
            last = cum[CHUNK - 1 : CHUNK]
            emid[at, :] = jnp.exp(cum - mid)
            k_mid = key[lo:hi] * jnp.exp(mid - cum)
            kmid[at, :] = k_mid.astype(bf16)
            k_end = (k_mid * jnp.exp(last - mid)).astype(bf16)
            held = state[...]
            old[chunk] = held.astype(bf16)
            stats[chunk, 0:1] = mid
            stats[chunk, 1:2] = offset[0:1, :]
            state[...] = held * jnp.exp(last) + dot(value[lo:hi], k_end, ((0,), (0,)))
            offset[...] += last
        return 0

    lax.fori_loop(0, nb, states, 0)

    def pack(slot, matrix, logs):
        hi, mid, low = split3(logs)
        slot[0:GROUP, :] = matrix.astype(bf16)
        r = lax.broadcasted_iota(jnp.int32, (LOGS, GROUP), 0)
        rows = jnp.where(r == 0, hi.astype(f32), jnp.where(r == 1, mid.astype(f32), low.astype(f32)))
        slot[GROUP : GROUP + LOGS, :] = rows.astype(bf16)

    def unpack(slot):
        logs = slot[GROUP : GROUP + LOGS, :].astype(f32)
        return slot[0:GROUP, :].astype(f32), logs[0:1] + logs[1:2] + logs[2:3]

    pack(ybuf.at[yy], state[...], offset[0:1, :])
    for r in range(1, ny):
        y_copy(r).start()

    for i in range(2, 6):
        w_copy(i).wait()
    taps_f = taps[...].astype(f32)

    def conv_block(t, _):
        here = rows_at(t)
        normed = tok[here, :]
        first = dot(normed, w[:, 2 * GROUP : 4 * GROUP])
        second = dot(normed, w[:, 4 * GROUP : 6 * GROUP])
        conv_in = first[:, :GROUP].astype(bf16).astype(f32) * first[:, GROUP:].astype(bf16).astype(f32)
        conv_in = conv_in.astype(bf16).astype(f32)
        proj_b = second[:, :GROUP].astype(bf16).astype(f32)
        gate[here, :] = second[:, GROUP:].astype(bf16)
        pad[HALO : HALO + ROWS, :] = conv_in
        total = taps_f[TAPS - 1 : TAPS] * conv_in
        for j in range(TAPS - 1):
            total += taps_f[j : j + 1] * pad[HALO - (TAPS - 1) + j : HALO - (TAPS - 1) + j + ROWS, :]
        put(1, t, (rms(proj_b * total) * group_gain[...]).astype(bf16))

        @pl.when(t == 0)
        def _():
            head_conv[...] = conv_in[:HALO]
            head_gate[...] = proj_b[:HALO]

        pad[0:HALO, :] = conv_in[ROWS - HALO :]

        @pl.when(t > 0)
        def _():
            for copy in own_copies(1, t):
                copy.start()

        return 0

    half = nb // 2
    lax.fori_loop(0, half, conv_block, 0)

    for r in range(1, ny):
        y_arrival(r).wait_recv()
    whole, logs = unpack(ybuf.at[0])
    for j in range(1, ny):
        more, log = unpack(ybuf.at[j])
        whole = whole * jnp.exp(log) + more
        logs = logs + log
    pack(zbuf.at[zz], whole, logs)

    def send_z(target, _):
        z_copy(target).start()
        return 0

    lax.fori_loop(zz + 1, nz, send_z, 0)

    lax.fori_loop(half, nb, conv_block, 0)
    tail[...] = pad[0:HALO, :]
    rim_copy.start()

    for kind in range(2):
        for k in range(tp - 2):
            far_cols_in(kind, k).wait_recv()
    for r in range(1, ny):
        for kind in range(2):
            for j in range(1, tp // 2):
                share_cols(kind, j, r).start()

    w_copy(6).wait()

    def reads(t, _):
        here = rows_at(t)

        @pl.when(t > 0)
        def _():
            relay_first(1, t)

        query = jax.nn.silu(dot(tok[here, :], w[:, 6 * GROUP : 7 * GROUP]).astype(bf16).astype(f32))
        for b in range(ROWS // CHUNK):
            lo, hi = b * CHUNK, (b + 1) * CHUNK
            at = pl.ds(pl.multiple_of(t * ROWS + lo, CHUNK), CHUNK)
            chunk = t * (ROWS // CHUNK) + b
            mid, before = stats[chunk, 0:1], stats[chunk, 1:2]
            q_mid = query[lo:hi] * emid[at, :]
            q_all = q_mid * jnp.exp(mid)
            qdev[at, :] = (q_all * jnp.exp(before)).astype(bf16)
            scores = dot(q_mid.astype(bf16), kmid[at, :], ((1,), (1,)))
            scores = jnp.where(causal, scores, 0.0).astype(bf16)
            read[at, :] = dot(scores, val[at, :]) + dot(q_all.astype(bf16), old[chunk], ((1,), (1,)))
        return 0

    lax.fori_loop(0, nb, reads, 0)

    rim_copy.wait_recv()
    before = jnp.where(place > 0, rim[...], 0.0)
    ext = jnp.concatenate([before, head_conv[...]], axis=0)
    fixed = taps_f[TAPS - 1 : TAPS] * head_conv[...]
    for j in range(TAPS - 1):
        fixed += taps_f[j : j + 1] * ext[HALO - (TAPS - 1) + j : 2 * HALO - (TAPS - 1) + j]
    fixed = rms(head_gate[...] * fixed) * group_gain[...]
    mixed[0, 0:HALO, pl.ds(pl.multiple_of((tp + me) * GROUP, GROUP), GROUP)] = fixed.astype(bf16)
    for copy in own_copies(1, 0):
        copy.start()

    incoming[...] = jnp.zeros_like(incoming)

    def hop_z(source, _):
        z_arrival(source).wait_recv()
        matrix, log = unpack(zbuf.at[source])
        incoming[...] = incoming[...] * jnp.exp(log) + matrix
        return 0

    lax.fori_loop(0, zz, hop_z, 0)

    def hop_y(source, _):
        matrix, log = unpack(ybuf.at[source])
        incoming[...] = incoming[...] * jnp.exp(log) + matrix
        return 0

    lax.fori_loop(0, yy, hop_y, 0)

    def merge(t, _):
        here = rows_at(t)
        total = read[here, :] + dot(qdev[here, :], incoming[...].astype(bf16), ((1,), (1,)))
        out = rms(total) * state_gain[...] * jax.nn.silu(gate[here, :].astype(f32))
        put(0, t, out.astype(bf16))
        for copy in own_copies(0, t):
            copy.start()
        return 0

    lax.fori_loop(0, nb, merge, 0)

    relay_first(1, 0)

    def relay_conv(t, _):
        relay_second(1, t + 1)
        return 0

    lax.fori_loop(0, nb - 1, relay_conv, 0)

    def relay_state(t, _):
        relay_first(0, t)
        return 0

    lax.fori_loop(0, nb, relay_state, 0)
    relay_second(1, 0)

    for kind in range(2):
        own_cols(kind).wait()
        partner_cols_in(kind).wait_recv()
        for r in range(1, ny):
            for j in range(1, tp // 2):
                share_cols_in(kind, j, r).wait_recv()

    def finish(t, _):
        relay_second(0, t)
        for kind in range(2):
            for k in range(tp // 2):
                arrival(kind, t, lax.rem(partner + 2 * k, tp)).wait_recv()
        result[rows_at(t), :] = dot(mixed[t], cols[...].reshape(2 * tp * GROUP, ncols)).astype(bf16)
        return 0

    lax.fori_loop(0, nb, finish, 0)

    def drain(t, _):
        for kind in range(2):
            for copy in own_copies(kind, t) + near_relays(kind, t) + [far_relay(kind, t)]:
                copy.wait_send()
        return 0

    lax.fori_loop(0, nb, drain, 0)
    for kind in range(2):
        partner_cols(kind).wait_send()
        for k in range(tp - 2):
            far_cols(kind, k).wait_send()
        for r in range(1, ny):
            for j in range(1, tp // 2):
                share_cols(kind, j, r).wait_send()
    for r in range(1, ny):
        y_copy(r).wait_send()

    def drain_z(target, _):
        z_copy(target).wait_send()
        return 0

    lax.fori_loop(zz + 1, nz, drain_z, 0)
    rim_copy.wait_send()


def body(
    tokens, in_gain, w_query, w_forget, w_input, w_outgate, w_conv_h, w_conv_b, w_conv_c,
    forget_floor, forget_leak, state_gain, conv_taps, group_gain, out_state, out_conv,
):
    count, feats = tokens.shape
    tp, sp = lax.axis_size("tp"), lax.axis_size("sp")
    ny, nz = NY, sp // NY
    ncols, nb = out_state.shape[1] // tp, count // ROWS
    nchunk = count // CHUNK
    hbm, vmem = pl.BlockSpec(memory_space=pl.ANY), pl.BlockSpec(memory_space=pltpu.VMEM)
    sems = pltpu.SemaphoreType.DMA
    return pl.pallas_call(
        functools.partial(fused_kernel, tp, ny, nz),
        in_specs=[hbm, vmem] + [hbm] * 7 + [vmem, hbm, vmem, vmem, vmem, hbm, hbm],
        out_specs=vmem,
        out_shape=jax.ShapeDtypeStruct((count, ncols), bf16),
        scratch_shapes=[
            pltpu.VMEM((count, feats), bf16),
            pltpu.VMEM((feats, 7 * GROUP), bf16),
            pltpu.VMEM((count, GROUP), f32),
            pltpu.VMEM((2 * tp, GROUP, ncols), bf16),
            pltpu.VMEM((nb, ROWS, 2 * tp * GROUP), bf16),
            pltpu.VMEM((count, GROUP), bf16),
            pltpu.VMEM((count, GROUP), bf16),
            pltpu.VMEM((count, GROUP), f32),
            pltpu.VMEM((nchunk, GROUP, GROUP), bf16),
            pltpu.VMEM((nchunk, HALO, GROUP), f32),
            pltpu.VMEM((count, GROUP), bf16),
            pltpu.VMEM((count, GROUP), f32),
            pltpu.VMEM((count, GROUP), bf16),
            pltpu.VMEM((HALO + ROWS, GROUP), f32),
            pltpu.VMEM((GROUP, GROUP), f32),
            pltpu.VMEM((HALO, GROUP), f32),
            pltpu.VMEM((GROUP, GROUP), f32),
            pltpu.VMEM((ny, GROUP + LOGS, GROUP), bf16),
            pltpu.VMEM((nz, GROUP + LOGS, GROUP), bf16),
            pltpu.VMEM((HALO, GROUP), f32),
            pltpu.VMEM((HALO, GROUP), f32),
            pltpu.VMEM((HALO, GROUP), f32),
            pltpu.VMEM((HALO, GROUP), f32),
            sems((nb,)), sems((7,)), sems((1,)), sems((2,)),
            sems((2, tp)), sems((2, tp)), sems((2, tp // 2, ny)), sems((2, tp // 2, ny)),
            sems((ny,)), sems((ny,)), sems((nz,)), sems((nz,)), sems((1,)), sems((1,)),
            sems((2, 7, nb)), sems((2, tp, nb)),
        ],
        compiler_params=pltpu.CompilerParams(
            vmem_limit_bytes=48 * 2**20, collective_id=0, has_side_effects=True
        ),
    )(
        tokens, in_gain[None], w_query, w_forget, w_input, w_outgate, w_conv_h, w_conv_b, w_conv_c,
        forget_floor[None], forget_leak, state_gain[None], conv_taps, group_gain[None],
        out_state, out_conv,
    )


def solution(mesh):
    cols, rows = P(None, "tp"), P("tp", None)
    in_specs = (
        P("sp", None), P(), cols, cols, cols, cols, cols, cols, cols,
        P("tp"), P("sp", "tp"), P(), cols, P(), rows, rows,
    )
    return jax.shard_map(
        body, mesh=mesh, in_specs=in_specs, out_specs=P("sp", "tp"), check_vma=False
    )
```

time: 77.8 us -> 60.6 us (0.78)
  Pallas kernels: 75.4 us -> 45.4 us
  local copies, waits for them, and re-layouts: 1.87 us -> 14.5 us
    pallas_call x1, Pallas kernels: 75.4 us -> 45.4 us  [body(): pl.pallas_call(functools.partial(fused_kernel, tp, ny, nz), in_specs=[hbm...]
    unnamed x1 -> x31, local copies, waits for them, and re-layouts: 1.87 us -> 14.5 us
where the time goes in v1:
time: 60.6 us; the launch traced here: 60 us
  Pallas kernels  45.4 us (75%)
  local copies, waits for them, and re-layouts  14.5 us (24%)
    pallas_call x1, Pallas kernels, body(): pl.pallas_call(functools.partial(fused_kernel, tp, ny, nz), in_specs=[hbm...  45.4 us
    unnamed x31, local copies, waits for them, and re-layouts  14.5 us

profile of v1, /device:TPU:1, one launch (start us, length us, event | category | flops | bytes accessed | tf_op | source)
XLA Modules:
  0.0 60.0 jit_solution(815417901657079384)
XLA Ops:
  0.0 0.0 copy-start
  0.0 1.0 %copy-done = bf16[2048,128]{1,0:T(8,128)(2,1)S(1)} copy-done((bf16[2048,128]{1,0:T(8,128)(2,1)S(1)}, bf16[2048,128]{1,0:T(8,128)(2,1)}, u32[]{:S(2)}) %copy-start) | copy-done | bytes 524312
  1.0 0.0 copy-start.1
  1.0 1.0 %copy-done.1 = bf16[2048,128]{1,0:T(8,128)(2,1)S(1)} copy-done((bf16[2048,128]{1,0:T(8,128)(2,1)S(1)}, bf16[2048,128]{1,0:T(8,128)(2,1)}, u32[]{:S(2)}) %copy-start.1) | copy-done | bytes 524312
  2.1 0.0 copy-start.2
  2.1 1.0 %copy-done.2 = bf16[2048,128]{1,0:T(8,128)(2,1)S(1)} copy-done((bf16[2048,128]{1,0:T(8,128)(2,1)S(1)}, bf16[2048,128]{1,0:T(8,128)(2,1)}, u32[]{:S(2)}) %copy-start.2) | copy-done | bytes 524312
  3.1 0.0 copy-start.3
  3.1 1.0 %copy-done.3 = bf16[2048,128]{1,0:T(8,128)(2,1)S(1)} copy-done((bf16[2048,128]{1,0:T(8,128)(2,1)S(1)}, bf16[2048,128]{1,0:T(8,128)(2,1)}, u32[]{:S(2)}) %copy-start.3) | copy-done | bytes 524312
  4.2 0.0 copy-start.4
  4.2 1.0 %copy-done.4 = bf16[2048,128]{1,0:T(8,128)(2,1)S(1)} copy-done((bf16[2048,128]{1,0:T(8,128)(2,1)S(1)}, bf16[2048,128]{1,0:T(8,128)(2,1)}, u32[]{:S(2)}) %copy-start.4) | copy-done | bytes 524312
  5.2 0.0 copy-start.5
  5.2 1.0 %copy-done.5 = bf16[2048,128]{1,0:T(8,128)(2,1)S(1)} copy-done((bf16[2048,128]{1,0:T(8,128)(2,1)S(1)}, bf16[2048,128]{1,0:T(8,128)(2,1)}, u32[]{:S(2)}) %copy-start.5) | copy-done | bytes 524312
  6.3 0.0 copy-start.6
  6.3 1.0 %copy-done.6 = bf16[2048,128]{1,0:T(8,128)(2,1)S(1)} copy-done((bf16[2048,128]{1,0:T(8,128)(2,1)S(1)}, bf16[2048,128]{1,0:T(8,128)(2,1)}, u32[]{:S(2)}) %copy-start.6) | copy-done | bytes 524312
  7.3 0.0 copy-start.7
  7.3 1.0 %copy-done.7 = f32[1024,128]{1,0:T(8,128)S(1)} copy-done((f32[1024,128]{1,0:T(8,128)S(1)}, f32[1024,128]{1,0:T(8,128)}, u32[]{:S(2)}) %copy-start.7) | copy-done | bytes 524312
  8.3 0.0 copy-start.8
  8.3 1.0 %copy-done.8 = bf16[128,2048]{1,0:T(8,128)(2,1)S(1)} copy-done((bf16[128,2048]{1,0:T(8,128)(2,1)S(1)}, bf16[128,2048]{1,0:T(8,128)(2,1)}, u32[]{:S(2)}) %copy-start.8) | copy-done | bytes 524312
  9.4 0.0 copy-start.9
  9.4 1.0 %copy-done.9 = bf16[128,2048]{1,0:T(8,128)(2,1)S(1)} copy-done((bf16[128,2048]{1,0:T(8,128)(2,1)S(1)}, bf16[128,2048]{1,0:T(8,128)(2,1)}, u32[]{:S(2)}) %copy-start.9) | copy-done | bytes 524312
  10.4 0.0 copy-start.10
  10.4 0.7 %copy-done.10 = f32[2048]{0:T(1024)S(1)} copy-done((f32[2048]{0:T(1024)S(1)}, f32[2048]{0:T(1024)}, u32[]{:S(2)}) %copy-start.10) | copy-done | bytes 8216
  11.1 0.0 copy-start.11
  11.1 0.7 %copy-done.11 = bf16[3,128]{1,0:T(4,128)(2,1)S(1)} copy-done((bf16[3,128]{1,0:T(4,128)(2,1)S(1)}, bf16[3,128]{1,0:T(4,128)(2,1)}, u32[]{:S(2)}) %copy-start.11) | copy-done | bytes 792
  11.8 0.0 copy-start.12
  11.8 0.7 %copy-done.12 = f32[128]{0:T(128)S(1)} copy-done((f32[128]{0:T(128)S(1)}, f32[128]{0:T(128)}, u32[]{:S(2)}) %copy-start.12) | copy-done | bytes 536
  12.5 0.0 copy-start.13
  12.5 0.7 %copy-done.13 = f32[128]{0:T(128)S(1)} copy-done((f32[128]{0:T(128)S(1)}, f32[128]{0:T(128)}, u32[]{:S(2)}) %copy-start.13) | copy-done | bytes 536
  13.1 0.0 copy-start.14
  13.1 0.7 %copy-done.14 = f32[128]{0:T(128)S(1)} copy-done((f32[128]{0:T(128)S(1)}, f32[128]{0:T(128)}, u32[]{:S(2)}) %copy-start.14) | copy-done | bytes 536
  13.8 45.4 %shard_map.154 = bf16[1024,256]{1,0:T(8,128)(2,1)S(1)} custom-call(bf16[1024,2048]{1,0:T(8,128)(2,1)} %tokens.1, f32[1,2048]{1,0:T(1,128)S(1)} %bitcast.4, bf16[2048,128]{1,0:T(8,128)(2,1)S(1)} %copy-done, bf16[2048,128]{1,0:T(8,128)(2,1)S(1)} %copy-done.1, bf16[2048,128]{1,0:T(8,128)(2,1)S(1)} %copy-done.2, bf16[2048,128]{1,0:T(8,128)(2,1)S(1)} %copy-done.3, ...), custom_call_target="tpu_custom_call" | custom-call | tf_op jit(solution)/shard_map/pallas_call | solution.py:484
  59.2 0.8 %copy.18 = bf16[1024,256]{1,0:T(8,128)(2,1)} copy(bf16[1024,256]{1,0:T(8,128)(2,1)S(1)} %shard_map.154) | data formatting | bytes 1048576
Async XLA Ops:
  0.0 1.0 %copy-start = (bf16[2048,128]{1,0:T(8,128)(2,1)S(1)}, bf16[2048,128]{1,0:T(8,128)(2,1)}, u32[]{:S(2)}) copy-start(bf16[2048,128]{1,0:T(8,128)(2,1)} %wq.1) | copy-start | bytes 1572868
  1.0 1.0 %copy-start.1 = (bf16[2048,128]{1,0:T(8,128)(2,1)S(1)}, bf16[2048,128]{1,0:T(8,128)(2,1)}, u32[]{:S(2)}) copy-start(bf16[2048,128]{1,0:T(8,128)(2,1)} %wf.1) | copy-start | bytes 1572868
  2.1 1.0 %copy-start.2 = (bf16[2048,128]{1,0:T(8,128)(2,1)S(1)}, bf16[2048,128]{1,0:T(8,128)(2,1)}, u32[]{:S(2)}) copy-start(bf16[2048,128]{1,0:T(8,128)(2,1)} %wi.1) | copy-start | bytes 1572868
  3.1 1.0 %copy-start.3 = (bf16[2048,128]{1,0:T(8,128)(2,1)S(1)}, bf16[2048,128]{1,0:T(8,128)(2,1)}, u32[]{:S(2)}) copy-start(bf16[2048,128]{1,0:T(8,128)(2,1)} %wg.1) | copy-start | bytes 1572868
  4.2 1.0 %copy-start.4 = (bf16[2048,128]{1,0:T(8,128)(2,1)S(1)}, bf16[2048,128]{1,0:T(8,128)(2,1)}, u32[]{:S(2)}) copy-start(bf16[2048,128]{1,0:T(8,128)(2,1)} %wh.1) | copy-start | bytes 1572868
  5.2 1.0 %copy-start.5 = (bf16[2048,128]{1,0:T(8,128)(2,1)S(1)}, bf16[2048,128]{1,0:T(8,128)(2,1)}, u32[]{:S(2)}) copy-start(bf16[2048,128]{1,0:T(8,128)(2,1)} %wb.1) | copy-start | bytes 1572868
  6.3 1.0 %copy-start.6 = (bf16[2048,128]{1,0:T(8,128)(2,1)S(1)}, bf16[2048,128]{1,0:T(8,128)(2,1)}, u32[]{:S(2)}) copy-start(bf16[2048,128]{1,0:T(8,128)(2,1)} %wc.1) | copy-start | bytes 1572868
  7.3 1.0 %copy-start.7 = (f32[1024,128]{1,0:T(8,128)S(1)}, f32[1024,128]{1,0:T(8,128)}, u32[]{:S(2)}) copy-start(f32[1024,128]{1,0:T(8,128)} %leak.1) | copy-start | bytes 1572868
  8.3 1.0 %copy-start.8 = (bf16[128,2048]{1,0:T(8,128)(2,1)S(1)}, bf16[128,2048]{1,0:T(8,128)(2,1)}, u32[]{:S(2)}) copy-start(bf16[128,2048]{1,0:T(8,128)(2,1)} %out_state.1) | copy-start | bytes 1572868
  9.4 1.0 %copy-start.9 = (bf16[128,2048]{1,0:T(8,128)(2,1)S(1)}, bf16[128,2048]{1,0:T(8,128)(2,1)}, u32[]{:S(2)}) copy-start(bf16[128,2048]{1,0:T(8,128)(2,1)} %out_conv.1) | copy-start | bytes 1572868
  10.4 0.7 %copy-start.10 = (f32[2048]{0:T(1024)S(1)}, f32[2048]{0:T(1024)}, u32[]{:S(2)}) copy-start(f32[2048]{0:T(1024)} %param.17) | copy-start | bytes 24580
  11.1 0.7 %copy-start.11 = (bf16[3,128]{1,0:T(4,128)(2,1)S(1)}, bf16[3,128]{1,0:T(4,128)(2,1)}, u32[]{:S(2)}) copy-start(bf16[3,128]{1,0:T(4,128)(2,1)} %taps.1) | copy-start | bytes 2308
  11.8 0.7 %copy-start.12 = (f32[128]{0:T(128)S(1)}, f32[128]{0:T(128)}, u32[]{:S(2)}) copy-start(f32[128]{0:T(128)} %param.25) | copy-start | bytes 1540
  12.5 0.7 %copy-start.13 = (f32[128]{0:T(128)S(1)}, f32[128]{0:T(128)}, u32[]{:S(2)}) copy-start(f32[128]{0:T(128)} %param.27) | copy-start | bytes 1540
  13.1 0.7 %copy-start.14 = (f32[128]{0:T(128)S(1)}, f32[128]{0:T(128)}, u32[]{:S(2)}) copy-start(f32[128]{0:T(128)} %param.29) | copy-start | bytes 1540

commit v2 on v1

v2 whole, which is shorter than its diff:
```python
import functools

import jax
import jax.numpy as jnp
from jax import lax
from jax.experimental import pallas as pl
from jax.experimental.pallas import tpu as pltpu
from jax.sharding import PartitionSpec as P

GROUP = 128
CHUNK = 128
ROWS = 256
TAPS = 3
HALO = 8
NY = 4
LOGS = 16

norm_eps = 1e-06
f32 = jnp.float32
bf16 = jnp.bfloat16


scope = jax.named_scope


def dot(a, b, dims=((1,), (0,))):
    return lax.dot_general(a, b, (dims, ((), ())), preferred_element_type=f32)


def rms(values):
    return values * lax.rsqrt(jnp.mean(values * values, axis=-1, keepdims=True) + norm_eps)


def split3(values):
    hi = values.astype(bf16)
    rest = values - hi.astype(f32)
    mid = rest.astype(bf16)
    low = (rest - mid.astype(f32)).astype(bf16)
    return hi, mid, low


def fused_kernel(
    tp, ny, nz,
    tokens, in_gain, wq, wf, wi, wg, wh, wb, wc, floor, leak, state_gain, taps, group_gain,
    out_state, out_conv, result,
    tok, w, leakv, cols, mixed, kmid, val, emid, old, stats, gate, read, qdev, scl, outv,
    gainv, floorv, sgainv, ggainv, tapsv,
    pad, incoming, ybuf, zbuf, rim, tail, head_gate,
    tok_sem, w_sem, small_sem, own_sem, out_sem, ready_z, ready_rim,
    colx_send, colx_recv, coly_send, coly_recv,
    y_send, y_recv, z_send, z_recv, rim_send, rim_recv, blk_send, blk_recv,
):
    me, place = lax.axis_index("tp"), lax.axis_index("sp")
    sp = ny * nz
    core, chip = lax.rem(me, 2), lax.div(me, 2)
    partner = me + 1 - 2 * core
    yy, zz = lax.rem(place, ny), lax.div(place, ny)
    far = lax.rem(me + 4, tp)
    ahead = lax.rem(me + tp + 2 - 4 * core, tp)
    behind = lax.rem(me + tp - 2 + 4 * core, tp)
    count, ncols = result.shape
    nb = count // ROWS
    nchunk = count // CHUNK
    part = GROUP // ny
    per = ROWS // CHUNK
    outs = (out_state, out_conv)

    def rows_at(t):
        return pl.ds(pl.multiple_of(t * ROWS, ROWS), ROWS)

    def tok_copy(t):
        return pltpu.make_async_copy(tokens.at[rows_at(t)], tok.at[rows_at(t)], tok_sem.at[t])

    weights = (wf, wi, wc, wh, wb, wg, wq)

    def w_copy(i):
        return pltpu.make_async_copy(weights[i], w.at[:, i * GROUP : (i + 1) * GROUP], w_sem.at[i])

    smalls = (
        pltpu.make_async_copy(in_gain, gainv, small_sem.at[0]),
        pltpu.make_async_copy(floor, floorv, small_sem.at[1]),
        pltpu.make_async_copy(leak, leakv, small_sem.at[2]),
        pltpu.make_async_copy(taps, tapsv, small_sem.at[3]),
        pltpu.make_async_copy(group_gain, ggainv, small_sem.at[4]),
        pltpu.make_async_copy(state_gain, sgainv, small_sem.at[5]),
    )

    def out_copy(t):
        return pltpu.make_async_copy(outv.at[rows_at(t)], result.at[rows_at(t)], out_sem.at[t])

    def col_slice(target):
        return pl.ds(pl.multiple_of(target * ncols, ncols), ncols)

    mine_rows = pl.ds(pl.multiple_of(yy * part, part), part)

    def own_cols(kind):
        return pltpu.make_async_copy(
            outs[kind].at[:, col_slice(me)], cols.at[kind * tp + me], own_sem.at[kind]
        )

    def partner_cols(kind):
        return pltpu.make_async_remote_copy(
            outs[kind].at[:, col_slice(partner)], cols.at[kind * tp + me],
            colx_send.at[kind, 0], colx_recv.at[kind, me], device_id={"tp": partner},
        )

    def partner_cols_in(kind):
        return pltpu.make_async_remote_copy(
            outs[kind].at[:, col_slice(partner)], cols.at[kind * tp + partner],
            colx_send.at[kind, 0], colx_recv.at[kind, partner], device_id={"tp": partner},
        )

    def far_cols(kind, k):
        target = lax.rem(2 * chip + 2 + k, tp)
        return pltpu.make_async_remote_copy(
            outs[kind].at[mine_rows, col_slice(target)], cols.at[kind * tp + me, mine_rows],
            colx_send.at[kind, k + 1], colx_recv.at[kind, me], device_id={"tp": target},
        )

    def far_cols_in(kind, k):
        source = lax.rem(2 * chip + 2 + k, tp)
        return pltpu.make_async_remote_copy(
            outs[kind].at[mine_rows, col_slice(source)], cols.at[kind * tp + source, mine_rows],
            colx_send.at[kind, k + 1], colx_recv.at[kind, source], device_id={"tp": source},
        )

    def share_cols(kind, j, r):
        pair = pl.ds(kind * tp + lax.rem(2 * chip + 2 * j, tp), 2)
        ref = cols.at[pair, mine_rows]
        peer = lax.rem(yy + r, ny)
        return pltpu.make_async_remote_copy(
            ref, ref, coly_send.at[kind, j, r], coly_recv.at[kind, j, yy],
            device_id={"sp": zz * ny + peer},
        )

    def share_cols_in(kind, j, r):
        pair = pl.ds(kind * tp + lax.rem(2 * chip + 2 * j, tp), 2)
        peer = lax.rem(yy + r, ny)
        ref = cols.at[pair, pl.ds(pl.multiple_of(peer * part, part), part)]
        return pltpu.make_async_remote_copy(
            ref, ref, coly_send.at[kind, j, r], coly_recv.at[kind, j, peer],
            device_id={"sp": zz * ny + peer},
        )

    def y_copy(r):
        ref = ybuf.at[yy]
        return pltpu.make_async_remote_copy(
            ref, ref, y_send.at[r], y_recv.at[yy],
            device_id={"sp": zz * ny + lax.rem(yy + r, ny)},
        )

    def y_arrival(r):
        peer = lax.rem(yy + r, ny)
        ref = ybuf.at[peer]
        return pltpu.make_async_remote_copy(
            ref, ref, y_send.at[r], y_recv.at[peer], device_id={"sp": zz * ny + peer}
        )

    def z_copy(target):
        ref = zbuf.at[zz]
        return pltpu.make_async_remote_copy(
            ref, ref, z_send.at[target], z_recv.at[zz], device_id={"sp": target * ny + yy}
        )

    def z_arrival(source):
        ref = zbuf.at[source]
        return pltpu.make_async_remote_copy(
            ref, ref, z_send.at[source], z_recv.at[source], device_id={"sp": source * ny + yy}
        )

    rim_copy = pltpu.make_async_remote_copy(
        tail, rim, rim_send.at[0], rim_recv.at[0], device_id={"sp": place + 1}
    )
    rim_arrival = pltpu.make_async_remote_copy(
        tail, rim, rim_send.at[0], rim_recv.at[0], device_id={"sp": place - 1}
    )

    def block_copy(kind, t, origin, target, slot):
        lanes = pl.ds(pl.multiple_of((kind * tp + origin) * GROUP, GROUP), GROUP)
        ref = mixed.at[t, :, lanes]
        return pltpu.make_async_remote_copy(
            ref, ref, blk_send.at[kind, slot, t], blk_recv.at[kind, origin, t],
            device_id={"tp": target},
        )

    def own_copies(kind, t):
        return [
            block_copy(kind, t, me, ahead, 1),
            block_copy(kind, t, me, behind, 2),
            block_copy(kind, t, me, partner, 0),
        ]

    def near_relays(kind, t):
        return [
            block_copy(kind, t, behind, ahead, 3),
            block_copy(kind, t, behind, partner, 4),
            block_copy(kind, t, ahead, partner, 5),
        ]

    def far_relay(kind, t):
        return block_copy(kind, t, far, partner, 6)

    def arrival(kind, t, origin):
        return block_copy(kind, t, origin, partner, 0)

    def relay_first(kind, t):
        first, second, third = near_relays(kind, t)
        arrival(kind, t, behind).wait_recv()
        first.start()
        second.start()
        arrival(kind, t, ahead).wait_recv()
        third.start()

    def relay_second(kind, t):
        arrival(kind, t, far).wait_recv()
        far_relay(kind, t).start()

    def put(kind, t, value):
        lanes = pl.ds(pl.multiple_of((kind * tp + me) * GROUP, GROUP), GROUP)
        mixed[t, :, lanes] = value

    smalls[0].start()
    tok_copy(0).start()
    w_copy(0).start()
    w_copy(1).start()
    smalls[1].start()
    smalls[2].start()
    for t in range(1, nb):
        tok_copy(t).start()
    barrier = pltpu.get_barrier_semaphore()
    for k in range(1, tp):
        pl.semaphore_signal(barrier, inc=1, device_id={"tp": lax.rem(me + k, tp)})
    for r in range(1, ny):
        pl.semaphore_signal(barrier, inc=1, device_id={"sp": zz * ny + lax.rem(yy + r, ny)})

    def greet_z(target, _):
        pl.semaphore_signal(barrier, inc=1, device_id={"sp": target * ny + yy})
        return 0

    lax.fori_loop(zz + 1, nz, greet_z, 0)

    @pl.when(place < sp - 1)
    def _():
        pl.semaphore_signal(barrier, inc=1, device_id={"sp": place + 1})

    for i in range(2, 7):
        w_copy(i).start()
    for copy in smalls[3:]:
        copy.start()
    with scope("barrier"):
        pl.semaphore_wait(barrier, tp + ny - 2 + zz + jnp.minimum(place, 1))

    def ready(target, _):
        pl.semaphore_signal(ready_z.at[0], inc=1, device_id={"sp": target * ny + yy})
        return 0

    lax.fori_loop(0, zz, ready, 0)

    @pl.when(place > 0)
    def _():
        pl.semaphore_signal(ready_rim.at[0], inc=1, device_id={"sp": place - 1})

    for kind in range(2):
        for k in range(tp - 2):
            far_cols(kind, k).start()
    for kind in range(2):
        partner_cols(kind).start()
        own_cols(kind).start()

    row = lax.broadcasted_iota(jnp.int32, (CHUNK, CHUNK), 0)
    col = lax.broadcasted_iota(jnp.int32, (CHUNK, CHUNK), 1)
    causal = row >= col
    ones = causal.astype(bf16)

    def lanes(first, last):
        return slice(first * GROUP, last * GROUP)

    def project_states(t):
        here = slice(t * ROWS, (t + 1) * ROWS)
        with scope("tokwait"):
            tok_copy(t).wait()
        raw = tok[here, :]
        scaled = raw * gainv[...].astype(bf16)
        tok[here, :] = scaled
        squares = raw * raw
        width = squares.shape[1] // 2
        squares = (squares[:, :width] + squares[:, width:]).astype(f32)
        mean = jnp.sum(squares, axis=1, keepdims=True) * (1.0 / raw.shape[1])
        scale = jnp.broadcast_to(lax.rsqrt(mean + norm_eps), (ROWS, GROUP))
        scl[here, :] = scale
        both = dot(scaled, w[:, lanes(0, 2)])
        x = (both[:, :GROUP] * scale).astype(bf16)
        value = (both[:, GROUP:] * scale).astype(bf16)
        return x, value

    def chain(t, x, value, carry):
        state, offset = carry
        val[slice(t * ROWS, (t + 1) * ROWS), :] = value
        key = (1.0 - floorv[...]) * jax.nn.sigmoid(-x.astype(f32))
        logf = jnp.log(1.0 - key) + leakv[slice(t * ROWS, (t + 1) * ROWS), :]
        for b in range(per):
            lo, hi = b * CHUNK, (b + 1) * CHUNK
            at = slice(t * ROWS + lo, t * ROWS + hi)
            chunk = t * per + b
            sums = dot(ones, jnp.concatenate(split3(logf[lo:hi]), axis=1))
            cum = sums[:, :GROUP] + sums[:, GROUP : 2 * GROUP] + sums[:, 2 * GROUP :]
            mid = cum[CHUNK // 2 - 1 : CHUNK // 2]
            last = cum[CHUNK - 1 : CHUNK]
            emid[at, :] = jnp.exp(cum - mid)
            k_mid = key[lo:hi] * jnp.exp(mid - cum)
            kmid[at, :] = k_mid.astype(bf16)
            k_end = (k_mid * jnp.exp(last - mid)).astype(bf16)
            old[chunk] = state.astype(bf16)
            stats[chunk, 0:1] = mid
            stats[chunk, 1:2] = offset
            state = state * jnp.exp(last) + dot(value[lo:hi], k_end, ((0,), (0,)))
            offset = offset + last
        return state, offset

    carry = (jnp.zeros((GROUP, GROUP), f32), jnp.zeros((1, GROUP), f32))
    with scope("w01wait"):
        smalls[0].wait()
        w_copy(0).wait()
        w_copy(1).wait()
    with scope("A"):
        held = project_states(0)
        smalls[1].wait()
        smalls[2].wait()
        for t in range(1, nb):
            more = project_states(t)
            carry = chain(t - 1, *held, carry)
            held = more
        carry = chain(nb - 1, *held, carry)

    def pack(slot, matrix, logs):
        hi, mid, low = split3(logs)
        slot[0:GROUP, :] = matrix.astype(bf16)
        r = lax.broadcasted_iota(jnp.int32, (LOGS, GROUP), 0)
        rows = jnp.where(r == 0, hi.astype(f32), jnp.where(r == 1, mid.astype(f32), low.astype(f32)))
        slot[GROUP : GROUP + LOGS, :] = rows.astype(bf16)

    def unpack(slot):
        logs = slot[GROUP : GROUP + LOGS, :].astype(f32)
        return slot[0:GROUP, :].astype(f32), logs[0:1] + logs[1:2] + logs[2:3]

    pack(ybuf.at[yy], *carry)
    for r in range(1, ny):
        y_copy(r).start()

    with scope("w23wait"):
        w_copy(2).wait()
        w_copy(3).wait()

    def gated_inputs(here):
        both = dot(tok[here, :], w[:, lanes(2, 4)])
        factor = scl[here, :]
        left = (both[:, :GROUP] * factor).astype(bf16).astype(f32)
        right = (both[:, GROUP:] * factor).astype(bf16).astype(f32)
        return (left * right).astype(bf16).astype(f32)

    with scope("rimsend"):
        tail[...] = gated_inputs(slice(count - 2 * HALO, count))[HALO:]

        @pl.when(place < sp - 1)
        def _():
            pl.semaphore_wait(ready_rim.at[0], 1)
            rim_copy.start()

    with scope("w45wait"):
        w_copy(4).wait()
        w_copy(5).wait()
        for copy in smalls[3:]:
            copy.wait()
    taps_f = tapsv[...].astype(f32)
    pad[0:HALO, :] = jnp.zeros((HALO, GROUP), f32)

    def convolve(first, size, conv_in, proj_b):
        total = taps_f[TAPS - 1 : TAPS] * conv_in
        for j in range(TAPS - 1):
            start = HALO - (TAPS - 1) + j + first
            total += taps_f[j : j + 1] * pad[start : start + size, :]
        return (rms(proj_b * total) * ggainv[...]).astype(bf16)

    def conv_block(t):
        here = slice(t * ROWS, (t + 1) * ROWS)
        conv_in = gated_inputs(here)
        pad[HALO + t * ROWS : HALO + (t + 1) * ROWS, :] = conv_in
        both = dot(tok[here, :], w[:, lanes(4, 6)])
        factor = scl[here, :]
        proj_b = (both[:, :GROUP] * factor).astype(bf16).astype(f32)
        gate[here, :] = (both[:, GROUP:] * factor).astype(bf16)
        if t == 0:
            head_gate[...] = proj_b[: 2 * HALO]
        put(1, t, convolve(t * ROWS, ROWS, conv_in, proj_b))

    def send(kind, t):
        for copy in own_copies(kind, t):
            copy.start()

    with scope("B01"):
        conv_block(0)
        conv_block(1)
        send(1, 1)

    with scope("rimwait"):
        @pl.when(place > 0)
        def _():
            rim_arrival.wait_recv()
            pad[0:HALO, :] = rim[...]

    fixed = convolve(0, 2 * HALO, pad[HALO : 3 * HALO, :], head_gate[...])
    mixed[0, 0 : 2 * HALO, pl.ds(pl.multiple_of((tp + me) * GROUP, GROUP), GROUP)] = fixed
    send(1, 0)

    with scope("ywait"):
        for r in range(1, ny):
            y_arrival(r).wait_recv()
    whole, logs = unpack(ybuf.at[0])
    for j in range(1, ny):
        more, log = unpack(ybuf.at[j])
        whole = whole * jnp.exp(log) + more
        logs = logs + log
    pack(zbuf.at[zz], whole, logs)
    with scope("readyz"):
        @pl.when(zz < nz - 1)
        def _():
            pl.semaphore_wait(ready_z.at[0], nz - 1 - zz)

    def send_z(target, _):
        z_copy(target).start()
        return 0

    lax.fori_loop(zz + 1, nz, send_z, 0)

    with scope("B23"):
        for t in range(2, nb):
            conv_block(t)
            send(1, t)

    with scope("colxwait"):
        for kind in range(2):
            for k in range(tp - 2):
                far_cols_in(kind, k).wait_recv()
    for r in range(1, ny):
        for kind in range(2):
            for j in range(1, tp // 2):
                share_cols(kind, j, r).start()

    with scope("w6wait"):
        w_copy(6).wait()

    def reads(t):
        here = slice(t * ROWS, (t + 1) * ROWS)
        x = (dot(tok[here, :], w[:, lanes(6, 7)]) * scl[here, :]).astype(bf16).astype(f32)
        query = jax.nn.silu(x)
        for b in range(per):
            lo, hi = b * CHUNK, (b + 1) * CHUNK
            at = slice(t * ROWS + lo, t * ROWS + hi)
            chunk = t * per + b
            mid, before = stats[chunk, 0:1], stats[chunk, 1:2]
            q_mid = query[lo:hi] * emid[at, :]
            q_all = q_mid * jnp.exp(mid)
            qdev[at, :] = (q_all * jnp.exp(before)).astype(bf16)
            scores = dot(q_mid.astype(bf16), kmid[at, :], ((1,), (1,)))
            scores = jnp.where(causal, scores, 0.0).astype(bf16)
            read[at, :] = dot(scores, val[at, :]) + dot(q_all.astype(bf16), old[chunk], ((1,), (1,)))

    with scope("C"):
        for t in range(nb):
            reads(t)

    conv_order = [1, 0] + list(range(2, nb))
    with scope("relayconv"):
        for t in conv_order[:-1]:
            relay_first(1, t)

    incoming[...] = jnp.zeros_like(incoming)

    def hop_z(source, _):
        with scope("zwait"):
            z_arrival(source).wait_recv()
        matrix, log = unpack(zbuf.at[source])
        incoming[...] = incoming[...] * jnp.exp(log) + matrix
        return 0

    with scope("hopz"):
        lax.fori_loop(0, zz, hop_z, 0)

    def hop_y(source, _):
        matrix, log = unpack(ybuf.at[source])
        incoming[...] = incoming[...] * jnp.exp(log) + matrix
        return 0

    lax.fori_loop(0, yy, hop_y, 0)

    def merge(t):
        here = slice(t * ROWS, (t + 1) * ROWS)
        total = read[here, :] + dot(qdev[here, :], incoming[...].astype(bf16), ((1,), (1,)))
        out = rms(total) * sgainv[...] * jax.nn.silu(gate[here, :].astype(f32))
        put(0, t, out.astype(bf16))
        send(0, t)

    with scope("merge"):
        for t in range(nb):
            merge(t)

    with scope("relayconvlast"):
        relay_first(1, conv_order[-1])
    with scope("relayconv2"):
        for t in conv_order[:-1]:
            relay_second(1, t)

    def relay_state(t, _):
        with scope("relaystate"):
            relay_first(0, t)
        return 0

    lax.fori_loop(0, nb, relay_state, 0)
    with scope("relayconv2last"):
        relay_second(1, conv_order[-1])

    with scope("colwait"):
        for kind in range(2):
            own_cols(kind).wait()
            partner_cols_in(kind).wait_recv()
            for r in range(1, ny):
                for j in range(1, tp // 2):
                    share_cols_in(kind, j, r).wait_recv()

    def finish(t, _):
        with scope("finfar"):
            relay_second(0, t)
        with scope("finwait"):
            for kind in range(2):
                for k in range(tp // 2):
                    arrival(kind, t, lax.rem(partner + 2 * k, tp)).wait_recv()
        outv[rows_at(t), :] = dot(mixed[t], cols[...].reshape(2 * tp * GROUP, ncols)).astype(bf16)
        out_copy(t).start()
        return 0

    lax.fori_loop(0, nb, finish, 0)

    def drain(t, _):
        for kind in range(2):
            for copy in own_copies(kind, t) + near_relays(kind, t) + [far_relay(kind, t)]:
                copy.wait_send()
        return 0

    with scope("drain"):
        lax.fori_loop(0, nb, drain, 0)
        for kind in range(2):
            partner_cols(kind).wait_send()
            for k in range(tp - 2):
                far_cols(kind, k).wait_send()
            for r in range(1, ny):
                for j in range(1, tp // 2):
                    share_cols(kind, j, r).wait_send()
        for r in range(1, ny):
            y_copy(r).wait_send()

        def drain_z(target, _):
            z_copy(target).wait_send()
            return 0

        lax.fori_loop(zz + 1, nz, drain_z, 0)

        @pl.when(place < sp - 1)
        def _():
            rim_copy.wait_send()

    with scope("outwait"):
        for t in range(nb):
            out_copy(t).wait()


def body(
    tokens, in_gain, w_query, w_forget, w_input, w_outgate, w_conv_h, w_conv_b, w_conv_c,
    forget_floor, forget_leak, state_gain, conv_taps, group_gain, out_state, out_conv,
):
    count, feats = tokens.shape
    tp, sp = lax.axis_size("tp"), lax.axis_size("sp")
    ny, nz = NY, sp // NY
    ncols, nb = out_state.shape[1] // tp, count // ROWS
    nchunk = count // CHUNK
    hbm, vmem = pl.BlockSpec(memory_space=pl.ANY), pl.BlockSpec(memory_space=pltpu.VMEM)
    sems = pltpu.SemaphoreType.DMA
    return pl.pallas_call(
        functools.partial(fused_kernel, tp, ny, nz),
        in_specs=[hbm] * 16,
        out_specs=hbm,
        out_shape=jax.ShapeDtypeStruct((count, ncols), bf16),
        scratch_shapes=[
            pltpu.VMEM((count, feats), bf16),
            pltpu.VMEM((feats, 7 * GROUP), bf16),
            pltpu.VMEM((count, GROUP), f32),
            pltpu.VMEM((2 * tp, GROUP, ncols), bf16),
            pltpu.VMEM((nb, ROWS, 2 * tp * GROUP), bf16),
            pltpu.VMEM((count, GROUP), bf16),
            pltpu.VMEM((count, GROUP), bf16),
            pltpu.VMEM((count, GROUP), f32),
            pltpu.VMEM((nchunk, GROUP, GROUP), bf16),
            pltpu.VMEM((nchunk, HALO, GROUP), f32),
            pltpu.VMEM((count, GROUP), bf16),
            pltpu.VMEM((count, GROUP), f32),
            pltpu.VMEM((count, GROUP), bf16),
            pltpu.VMEM((count, GROUP), f32),
            pltpu.VMEM((count, ncols), bf16),
            pltpu.VMEM((1, feats), f32),
            pltpu.VMEM((1, GROUP), f32),
            pltpu.VMEM((1, GROUP), f32),
            pltpu.VMEM((1, GROUP), f32),
            pltpu.VMEM((TAPS, GROUP), bf16),
            pltpu.VMEM((HALO + count, GROUP), f32),
            pltpu.VMEM((GROUP, GROUP), f32),
            pltpu.VMEM((ny, GROUP + LOGS, GROUP), bf16),
            pltpu.VMEM((nz, GROUP + LOGS, GROUP), bf16),
            pltpu.VMEM((HALO, GROUP), f32),
            pltpu.VMEM((HALO, GROUP), f32),
            pltpu.VMEM((2 * HALO, GROUP), f32),
            sems((nb,)), sems((7,)), sems((6,)), sems((2,)), sems((nb,)),
            pltpu.SemaphoreType.REGULAR((1,)), pltpu.SemaphoreType.REGULAR((1,)),
            sems((2, tp)), sems((2, tp)), sems((2, tp // 2, ny)), sems((2, tp // 2, ny)),
            sems((ny,)), sems((ny,)), sems((nz,)), sems((nz,)), sems((1,)), sems((1,)),
            sems((2, 7, nb)), sems((2, tp, nb)),
        ],
        compiler_params=pltpu.CompilerParams(
            vmem_limit_bytes=67043328, collective_id=0, has_side_effects=True
        ),
    )(
        tokens, in_gain[None], w_query, w_forget, w_input, w_outgate, w_conv_h, w_conv_b, w_conv_c,
        forget_floor[None], forget_leak, state_gain[None], conv_taps, group_gain[None],
        out_state, out_conv,
    )


def solution(mesh):
    cols, rows = P(None, "tp"), P("tp", None)
    in_specs = (
        P("sp", None), P(), cols, cols, cols, cols, cols, cols, cols,
        P("tp"), P("sp", "tp"), P(), cols, P(), rows, rows,
    )
    return jax.shard_map(
        body, mesh=mesh, in_specs=in_specs, out_specs=P("sp", "tp"), check_vma=False
    )
```

time: 60.6 us -> 39.8 us (0.66)
  the two profiles are of different devices: /device:TPU:1 before, /device:TPU:192 now
where the time goes in v2:
time: 39.8 us; the launch traced here: 39.7 us
  Pallas kernels  37.8 us (95%)
  local copies, waits for them, and re-layouts  1.87 us (5%)
    pallas_call x1, Pallas kernels, body(): pl.pallas_call(functools.partial(fused_kernel, tp, ny, nz), in_specs=[hbm...  37.8 us
    unnamed x1, local copies, waits for them, and re-layouts  1.87 us

profile of v2, /device:TPU:192, one launch (start us, length us, event | category | flops | bytes accessed | tf_op | source)
XLA Modules:
  0.0 39.7 jit_solution(13793228042786920934)
XLA Ops:
  0.0 37.8 %shard_map.154 = bf16[1024,256]{1,0:T(8,128)(2,1)} custom-call(bf16[1024,2048]{1,0:T(8,128)(2,1)} %tokens.1, f32[1,2048]{1,0:T(1,128)} %bitcast.4, bf16[2048,128]{1,0:T(8,128)(2,1)} %wq.1, bf16[2048,128]{1,0:T(8,128)(2,1)} %wf.1, bf16[2048,128]{1,0:T(8,128)(2,1)} %wi.1, bf16[2048,128]{1,0:T(8,128)(2,1)} %wg.1, bf16[2048,128]{1,0:T(8,128)(2,1)} %wh.1, ...), custom_call_target="tpu_custom_call" | custom-call | tf_op jit(solution)/shard_map/pallas_call | solution.py:587
  37.9 1.9 %copy.18 = bf16[1024,256]{1,0:T(8,128)(2,1)} copy(bf16[1024,256]{1,0:T(8,128)(2,1)} %shard_map.154) | data formatting | bytes 1048576

commit v3 on v2

v3 whole, which is shorter than its diff:
```python
import functools

import jax
import jax.numpy as jnp
from jax import lax
from jax.experimental import pallas as pl
from jax.experimental.pallas import tpu as pltpu
from jax.sharding import PartitionSpec as P

GROUP = 128
CHUNK = 128
ROWS = 256
TAPS = 3
HALO = 8
NY = 4
LOGS = 16
STRIP = 16

norm_eps = 1e-06
f32 = jnp.float32
bf16 = jnp.bfloat16


scope = jax.named_scope


def dot(a, b, dims=((1,), (0,))):
    return lax.dot_general(a, b, (dims, ((), ())), preferred_element_type=f32)


def rms(values):
    return values * lax.rsqrt(jnp.mean(values * values, axis=-1, keepdims=True) + norm_eps)


def split(values):
    hi = values.astype(bf16)
    return hi, (values - hi.astype(f32)).astype(bf16)


def fused_kernel(
    tp, ny, nz,
    tokens, in_gain, wq, wf, wi, wg, wh, wb, wc, floor, leak, state_gain, taps, group_gain,
    out_state, out_conv, result,
    tok, w, leakv, cols, mixed, xs, kmid, val, emid, old, stats, gate, read, qdev, scl, acc,
    gainv, floorv, sgainv, ggainv, tapsv, prods, wide,
    pad, incoming, ybuf, zbuf, rim, tail,
    tok_sem, w_sem, small_sem, own_sem, ready_z, ready_rim,
    colx_send, colx_recv, coly_send, coly_recv,
    y_send, y_recv, z_send, z_recv, rim_send, rim_recv, blk_send, near_recv, far_recv, pair_recv,
):
    me, place = lax.axis_index("tp"), lax.axis_index("sp")
    sp = ny * nz
    core, chip = lax.rem(me, 2), lax.div(me, 2)
    partner = me + 1 - 2 * core
    yy, zz = lax.rem(place, ny), lax.div(place, ny)
    far = lax.rem(me + 4, tp)
    ahead = lax.rem(me + tp + 2 - 4 * core, tp)
    behind = lax.rem(me + tp - 2 + 4 * core, tp)
    y_ahead = lax.rem(yy + ny + 1 - 2 * core, ny)
    y_behind = lax.rem(yy + ny - 1 + 2 * core, ny)
    count, ncols = result.shape
    nb = count // ROWS
    nchunk = count // CHUNK
    part = GROUP // ny
    per = ROWS // CHUNK
    outs = (out_state, out_conv)

    def rows_at(t):
        return pl.ds(pl.multiple_of(t * ROWS, ROWS), ROWS)

    def tok_copy(t):
        return pltpu.make_async_copy(tokens.at[rows_at(t)], tok.at[rows_at(t)], tok_sem.at[t])

    weights = (wf, wi, wc, wh, wb, wg, wq)

    def w_copy(i):
        return pltpu.make_async_copy(
            weights[i], w.at[:, i * GROUP : (i + 1) * GROUP], w_sem.at[i // 2]
        )

    def w_wait(first, last):
        ref = w.at[:, first * GROUP : last * GROUP]
        pltpu.make_async_copy(ref, ref, w_sem.at[first // 2]).wait()

    smalls = (
        pltpu.make_async_copy(in_gain, gainv, small_sem.at[0]),
        pltpu.make_async_copy(floor, floorv, small_sem.at[1]),
        pltpu.make_async_copy(leak, leakv, small_sem.at[2]),
        pltpu.make_async_copy(taps, tapsv, small_sem.at[3]),
        pltpu.make_async_copy(group_gain, ggainv, small_sem.at[4]),
        pltpu.make_async_copy(state_gain, sgainv, small_sem.at[5]),
    )

    def col_slice(target):
        return pl.ds(pl.multiple_of(target * ncols, ncols), ncols)

    mine_rows = pl.ds(pl.multiple_of(yy * part, part), part)

    def landed(ref, send, recv):
        return pltpu.make_async_remote_copy(ref, ref, send, recv, device_id={"tp": partner})

    def own_cols(kind):
        return pltpu.make_async_copy(
            outs[kind].at[:, col_slice(me)], cols.at[kind * tp + me], own_sem.at[0]
        )

    own_cols_done = pltpu.make_async_copy(
        cols.at[pl.ds(0, 2)], cols.at[pl.ds(0, 2)], own_sem.at[0]
    )

    def partner_cols(kind):
        return pltpu.make_async_remote_copy(
            outs[kind].at[:, col_slice(partner)], cols.at[kind * tp + me],
            colx_send.at[0], colx_recv.at[1], device_id={"tp": partner},
        )

    def far_cols(kind, k):
        target = lax.rem(2 * chip + 2 + k, tp)
        return pltpu.make_async_remote_copy(
            outs[kind].at[mine_rows, col_slice(target)], cols.at[kind * tp + me, mine_rows],
            colx_send.at[0], colx_recv.at[0], device_id={"tp": target},
        )

    far_units = 2 * (tp - 2) // ny
    far_cols_in = landed(cols.at[pl.ds(0, far_units)], colx_send.at[0], colx_recv.at[0])
    partner_cols_in = landed(cols.at[pl.ds(0, 2)], colx_send.at[0], colx_recv.at[1])
    colx_sent = landed(cols.at[pl.ds(0, far_units + 2)], colx_send.at[0], colx_recv.at[0])

    def share_cols(kind, j, origin, target, slot):
        pair = pl.ds(kind * tp + lax.rem(2 * chip + 2 * j, tp), 2)
        ref = cols.at[pair, pl.ds(pl.multiple_of(origin * part, part), part)]
        return pltpu.make_async_remote_copy(
            ref, ref, coly_send.at[0], coly_recv.at[slot], device_id={"sp": zz * ny + target}
        )

    def share_all(origin, target, slot):
        for kind in range(2):
            for j in range(1, tp // 2):
                share_cols(kind, j, origin, target, slot).start()

    def shared_in(slot):
        return landed(cols.at[pl.ds(0, far_units)], coly_send.at[0], coly_recv.at[slot])

    shares_sent = landed(cols.at[pl.ds(0, 3 * far_units)], coly_send.at[0], coly_recv.at[0])

    def y_copy(r):
        ref = ybuf.at[yy]
        return pltpu.make_async_remote_copy(
            ref, ref, y_send.at[0], y_recv.at[0],
            device_id={"sp": zz * ny + lax.rem(yy + r, ny)},
        )

    y_all = landed(ybuf.at[pl.ds(0, ny - 1)], y_send.at[0], y_recv.at[0])

    def z_copy(target):
        ref = zbuf.at[zz]
        return pltpu.make_async_remote_copy(
            ref, ref, z_send.at[target], z_recv.at[zz], device_id={"sp": target * ny + yy}
        )

    def z_arrival(source):
        ref = zbuf.at[source]
        return pltpu.make_async_remote_copy(
            ref, ref, z_send.at[source], z_recv.at[source], device_id={"sp": source * ny + yy}
        )

    rim_copy = pltpu.make_async_remote_copy(
        tail, rim, rim_send.at[0], rim_recv.at[0], device_id={"sp": place + 1}
    )
    rim_arrival = pltpu.make_async_remote_copy(
        tail, rim, rim_send.at[0], rim_recv.at[0], device_id={"sp": place - 1}
    )

    def block_copy(kind, t, origin, target, recv):
        lanes = pl.ds(pl.multiple_of((kind * tp + origin) * GROUP, GROUP), GROUP)
        ref = mixed.at[t, :, lanes]
        return pltpu.make_async_remote_copy(
            ref, ref, blk_send.at[0], recv.at[kind, t], device_id={"tp": target}
        )

    def relay_first(kind, t):
        landed(mixed.at[t, :, 0 : 2 * GROUP], blk_send.at[0], near_recv.at[kind, t]).wait_recv()
        block_copy(kind, t, behind, ahead, far_recv).start()
        block_copy(kind, t, behind, partner, pair_recv).start()
        block_copy(kind, t, ahead, partner, pair_recv).start()

    def relay_second(kind, t):
        landed(mixed.at[t, :, 0:GROUP], blk_send.at[0], far_recv.at[kind, t]).wait_recv()
        block_copy(kind, t, far, partner, pair_recv).start()

    def pair_wait(kind, t):
        half = mixed.at[t, :, 0 : tp // 2 * GROUP]
        landed(half, blk_send.at[0], pair_recv.at[kind, t]).wait_recv()

    blocks_sent = landed(
        mixed.at[:, :, 0 : 2 * (tp - 1) * GROUP], blk_send.at[0], pair_recv.at[0, 0]
    )

    def put(kind, t, value):
        lanes = pl.ds(pl.multiple_of((kind * tp + me) * GROUP, GROUP), GROUP)
        mixed[t, :, lanes] = value

    smalls[0].start()
    tok_copy(0).start()
    w_copy(0).start()
    w_copy(1).start()
    smalls[1].start()
    barrier = pltpu.get_barrier_semaphore()
    for k in range(1, tp):
        pl.semaphore_signal(barrier, inc=1, device_id={"tp": lax.rem(me + k, tp)})
    for r in range(1, ny):
        pl.semaphore_signal(barrier, inc=1, device_id={"sp": zz * ny + lax.rem(yy + r, ny)})

    def greet_z(target, _):
        pl.semaphore_signal(barrier, inc=1, device_id={"sp": target * ny + yy})
        return 0

    lax.fori_loop(zz + 1, nz, greet_z, 0)

    @pl.when(jnp.logical_and(yy == ny - 1, zz < nz - 1))
    def _():
        pl.semaphore_signal(barrier, inc=1, device_id={"sp": place + 1})

    def meet():
        with scope("barrier"):
            across = jnp.where(yy == 0, jnp.minimum(zz, 1), 0)
            pl.semaphore_wait(barrier, tp + ny - 2 + zz + across)

        def ready(target, _):
            pl.semaphore_signal(ready_z.at[0], inc=1, device_id={"sp": target * ny + yy})
            return 0

        lax.fori_loop(0, zz, ready, 0)

        @pl.when(jnp.logical_and(yy == 0, zz > 0))
        def _():
            pl.semaphore_signal(ready_rim.at[0], inc=1, device_id={"sp": place - 1})

        for kind in range(2):
            for k in range(tp - 2):
                far_cols(kind, k).start()
        for kind in range(2):
            partner_cols(kind).start()
            own_cols(kind).start()

    row = lax.broadcasted_iota(jnp.int32, (CHUNK, CHUNK), 0)
    col = lax.broadcasted_iota(jnp.int32, (CHUNK, CHUNK), 1)
    causal = row >= col
    ones = causal.astype(bf16)

    def lanes(first, last):
        return slice(first * GROUP, last * GROUP)

    def span(t):
        return slice(t * ROWS, (t + 1) * ROWS)

    def prepare(t):
        gain = gainv[...].astype(bf16)
        for r in range(t * ROWS, (t + 1) * ROWS, STRIP):
            raw = tok[r : r + STRIP, :]
            feats = raw.shape[1]
            tok[r : r + STRIP, :] = raw * gain
            squares = raw * raw
            squares = squares[:, : feats // 2] + squares[:, feats // 2 :]
            squares = squares[:, : feats // 4] + squares[:, feats // 4 :]
            mean = jnp.sum(squares.astype(f32), axis=1, keepdims=True) * (1.0 / feats)
            scl[r : r + STRIP, :] = jnp.broadcast_to(lax.rsqrt(mean + norm_eps), (STRIP, GROUP))

    def project_states(t):
        here = span(t)
        both = dot(tok[here, :], w[:, lanes(0, 2)])
        scale = scl[here, :]
        xs[here, :] = (both[:, :GROUP] * scale).astype(bf16)
        val[here, :] = (both[:, GROUP:] * scale).astype(bf16)

    def chain(t, carry):
        state, offset = carry
        here = span(t)
        key = (1.0 - floorv[...]) * jax.nn.sigmoid(-xs[here, :].astype(f32))
        terms = split(jnp.log(1.0 - key) + leakv[here, :])
        cums = []
        for b in range(per):
            rows = slice(b * CHUNK, (b + 1) * CHUNK)
            sums = dot(ones, jnp.concatenate([term[rows] for term in terms], axis=1))
            cums.append(sums[:, :GROUP] + sums[:, GROUP:])
        fresh = []
        for b in range(per):
            chunk, cum = t * per + b, cums[b]
            at = slice(chunk * CHUNK, (chunk + 1) * CHUNK)
            mid = cum[CHUNK // 2 - 1 : CHUNK // 2]
            last = cum[CHUNK - 1 : CHUNK]
            emid[at, :] = jnp.exp(cum - mid)
            k_mid = key[b * CHUNK : (b + 1) * CHUNK] * jnp.exp(mid - cum)
            kmid[at, :] = k_mid.astype(bf16)
            k_end = (k_mid * jnp.exp(last - mid)).astype(bf16)
            stats[chunk, 0:1] = mid
            fresh.append(dot(val[at, :], k_end, ((0,), (0,))))
        for b in range(per):
            chunk, last = t * per + b, cums[b][CHUNK - 1 : CHUNK]
            old[chunk] = state.astype(bf16)
            stats[chunk, 1:2] = offset
            state = state * jnp.exp(last) + fresh[b]
            offset = offset + last
        return state, offset

    def gated_inputs(both, factor):
        left = (both[:, :GROUP] * factor).astype(bf16).astype(f32)
        right = (both[:, GROUP:] * factor).astype(bf16).astype(f32)
        return (left * right).astype(bf16).astype(f32)

    carry = (jnp.zeros((GROUP, GROUP), f32), jnp.zeros((1, GROUP), f32))
    with scope("load0"):
        smalls[0].wait()
        tok_copy(0).wait()
    smalls[2].start()
    for t in range(1, nb):
        tok_copy(t).start()
    for i in range(2, 7):
        w_copy(i).start()
    for copy in smalls[3:]:
        copy.start()
    with scope("prep0"):
        prepare(0)
    with scope("load1"):
        w_wait(0, 2)
        smalls[1].wait()
    with scope("A"):
        project_states(0)
        smalls[2].wait()
        for t in range(1, nb):
            with scope("tokwait"):
                tok_copy(t).wait()
            prepare(t)
            carry = chain(t - 1, carry)
            project_states(t)
            if t == 1:
                meet()

    with scope("w23wait"):
        w_wait(2, 4)
    with scope("rimsend"):
        end = slice(count - 2 * HALO, count)
        tail[...] = gated_inputs(dot(tok[end, :], w[:, lanes(2, 4)]), scl[end, :])[HALO:]

        @pl.when(jnp.logical_and(yy == ny - 1, zz < nz - 1))
        def _():
            pl.semaphore_wait(ready_rim.at[0], 1)

        @pl.when(place < sp - 1)
        def _():
            rim_copy.start()

    with scope("A2"):
        carry = chain(nb - 1, carry)

    def pack(slot, matrix, logs):
        hi = logs.astype(bf16)
        mid, low = split(logs - hi.astype(f32))
        slot[0:GROUP, :] = matrix.astype(bf16)
        r = lax.broadcasted_iota(jnp.int32, (LOGS, GROUP), 0)
        rows = jnp.where(r == 0, hi.astype(f32), jnp.where(r == 1, mid.astype(f32), low.astype(f32)))
        slot[GROUP : GROUP + LOGS, :] = rows.astype(bf16)

    def unpack(slot):
        logs = slot[GROUP : GROUP + LOGS, :].astype(f32)
        return slot[0:GROUP, :].astype(f32), logs[0:1] + logs[1:2] + logs[2:3]

    pack(ybuf.at[yy], *carry)
    for r in range(1, ny):
        y_copy(r).start()

    with scope("w46wait"):
        w_wait(4, 6)
        w_wait(6, 7)
        for copy in smalls[3:]:
            copy.wait()
    taps_f = tapsv[...].astype(f32)
    pad[0:HALO, :] = jnp.zeros((HALO, GROUP), f32)

    def convolve(first, size, conv_in, proj_b):
        total = taps_f[TAPS - 1 : TAPS] * conv_in
        for j in range(TAPS - 1):
            start = HALO - (TAPS - 1) + j + first
            total += taps_f[j : j + 1] * pad[start : start + size, :]
        return (rms(proj_b * total) * ggainv[...]).astype(bf16)

    def project_inputs(t):
        here = span(t)
        pad[HALO + t * ROWS : HALO + (t + 1) * ROWS, :] = gated_inputs(
            dot(tok[here, :], w[:, lanes(2, 4)]), scl[here, :]
        )

    def project_gates(t):
        here = span(t)
        both = dot(tok[here, :], w[:, lanes(4, 6)])
        factor = scl[here, :]
        prods[here, :] = (both[:, :GROUP] * factor).astype(bf16)
        gate[here, :] = (both[:, GROUP:] * factor).astype(bf16)

    def project_query(t):
        here = span(t)
        wide[here, :] = (dot(tok[here, :], w[:, lanes(6, 7)]) * scl[here, :]).astype(bf16)

    def send(kind, t):
        block_copy(kind, t, me, ahead, near_recv).start()
        block_copy(kind, t, me, behind, near_recv).start()
        block_copy(kind, t, me, partner, pair_recv).start()

    def conv(t):
        conv_in = pad[HALO + t * ROWS : HALO + (t + 1) * ROWS, :]
        put(1, t, convolve(t * ROWS, ROWS, conv_in, prods[span(t), :].astype(f32)))

    def reads(chunk):
        at = slice(chunk * CHUNK, (chunk + 1) * CHUNK)
        query = jax.nn.silu(wide[at, :].astype(f32))
        mid, before = stats[chunk, 0:1], stats[chunk, 1:2]
        q_mid = query * emid[at, :]
        q_all = q_mid * jnp.exp(mid)
        qdev[at, :] = (q_all * jnp.exp(before)).astype(bf16)
        scores = dot(q_mid.astype(bf16), kmid[at, :], ((1,), (1,)))
        scores = jnp.where(causal, scores, 0.0).astype(bf16)
        read[at, :] = dot(scores, val[at, :]) + dot(q_all.astype(bf16), old[chunk], ((1,), (1,)))

    def combine():
        with scope("ywait"):
            y_all.wait_recv()
        whole, logs = unpack(ybuf.at[0])
        for j in range(1, ny):
            more, log = unpack(ybuf.at[j])
            whole = whole * jnp.exp(log) + more
            logs = logs + log
        pack(zbuf.at[zz], whole, logs)
        with scope("readyz"):
            @pl.when(zz < nz - 1)
            def _():
                pl.semaphore_wait(ready_z.at[0], nz - 1 - zz)

        def send_z(target, _):
            z_copy(target).start()
            return 0

        lax.fori_loop(zz + 1, nz, send_z, 0)

    def first_rows():
        with scope("rimwait"):
            @pl.when(place > 0)
            def _():
                rim_arrival.wait_recv()
                pad[0:HALO, :] = rim[...]

        conv(0)
        send(1, 0)

    def share():
        with scope("colxwait"):
            far_cols_in.wait_recv()
        share_all(yy, y_ahead, 0)
        share_all(yy, y_behind, 1)

    def share_on():
        with scope("colywait"):
            shared_in(0).wait_recv()
        share_all(y_behind, y_ahead, 2)

    with scope("B"):
        project_inputs(0)
        project_inputs(1)
        project_gates(1)
        conv(1)
        send(1, 1)
        project_gates(0)
        first_rows()
    share()
    combine()
    with scope("B2"):
        project_inputs(2)
        project_gates(2)
        conv(2)
        project_query(0)
        send(1, 2)
    with scope("B3"):
        project_inputs(3)
        project_gates(3)
        conv(3)
        project_query(1)
        reads(0)
        reads(1)
        send(1, 3)
    with scope("C2"):
        project_query(2)
        reads(2)
        reads(3)
        project_query(3)
        reads(4)
        reads(5)
    with scope("C3"):
        reads(6)
        reads(7)

    share_on()
    conv_order = [1, 0] + list(range(2, nb))
    with scope("relayconv"):
        for t in conv_order[:-1]:
            relay_first(1, t)

    incoming[...] = jnp.zeros_like(incoming)

    def hop_z(source, _):
        z_arrival(source).wait_recv()
        matrix, log = unpack(zbuf.at[source])
        incoming[...] = incoming[...] * jnp.exp(log) + matrix
        return 0

    with scope("hopz"):
        lax.fori_loop(0, zz, hop_z, 0)

    def hop_y(source, _):
        matrix, log = unpack(ybuf.at[source])
        incoming[...] = incoming[...] * jnp.exp(log) + matrix
        return 0

    lax.fori_loop(0, yy, hop_y, 0)

    def merge(t):
        here = span(t)
        total = read[here, :] + dot(qdev[here, :], incoming[...].astype(bf16), ((1,), (1,)))
        out = rms(total) * sgainv[...] * jax.nn.silu(gate[here, :].astype(f32))
        put(0, t, out.astype(bf16))
        send(0, t)

    with scope("merge"):
        for t in range(nb):
            merge(t)

    def conv_dot(t):
        with scope("convdot"):
            pair_wait(1, t)
            side = cols[tp : 2 * tp].reshape(tp * GROUP, ncols)
            acc[span(t), :] = dot(mixed[t, :, tp * GROUP :], side)

    with scope("relayconvlast"):
        relay_first(1, conv_order[-1])
    for t in range(nb - 1):
        with scope("relaystate"):
            relay_first(0, t)
        with scope("relayconv2"):
            relay_second(1, conv_order[t])
    with scope("colwait"):
        own_cols_done.wait()
        partner_cols_in.wait_recv()
        shared_in(1).wait_recv()
        shared_in(2).wait_recv()
    for t in conv_order[:-1]:
        conv_dot(t)
    with scope("relaystate"):
        relay_first(0, nb - 1)
    with scope("relayconv2last"):
        relay_second(1, conv_order[-1])

    def finish(t):
        with scope("finwait"):
            pair_wait(0, t)
        with scope("findot"):
            total = acc[span(t), :] + dot(mixed[t, :, : tp * GROUP], cols[0:tp].reshape(tp * GROUP, ncols))
            result[span(t), :] = total.astype(bf16)

    for t in range(nb):
        with scope("finfar"):
            relay_second(0, t)
        if t == 0:
            conv_dot(conv_order[-1])
        else:
            finish(t - 1)
    finish(nb - 1)

    with scope("drain"):
        blocks_sent.wait_send()
        colx_sent.wait_send()
        shares_sent.wait_send()
        y_all.wait_send()

        def drain_z(target, _):
            z_copy(target).wait_send()
            return 0

        lax.fori_loop(zz + 1, nz, drain_z, 0)

        @pl.when(place < sp - 1)
        def _():
            rim_copy.wait_send()


def body(
    tokens, in_gain, w_query, w_forget, w_input, w_outgate, w_conv_h, w_conv_b, w_conv_c,
    forget_floor, forget_leak, state_gain, conv_taps, group_gain, out_state, out_conv,
):
    count, feats = tokens.shape
    tp, sp = lax.axis_size("tp"), lax.axis_size("sp")
    ny, nz = NY, sp // NY
    ncols, nb = out_state.shape[1] // tp, count // ROWS
    nchunk = count // CHUNK
    hbm, vmem = pl.BlockSpec(memory_space=pltpu.HBM), pl.BlockSpec(memory_space=pltpu.VMEM)
    sems = pltpu.SemaphoreType.DMA
    return pl.pallas_call(
        functools.partial(fused_kernel, tp, ny, nz),
        in_specs=[hbm] * 16,
        out_specs=vmem,
        out_shape=jax.ShapeDtypeStruct((count, ncols), bf16),
        scratch_shapes=[
            pltpu.VMEM((count, feats), bf16),
            pltpu.VMEM((feats, 7 * GROUP), bf16),
            pltpu.VMEM((count, GROUP), f32),
            pltpu.VMEM((2 * tp, GROUP, ncols), bf16),
            pltpu.VMEM((nb, ROWS, 2 * tp * GROUP), bf16),
            pltpu.VMEM((count, GROUP), bf16),
            pltpu.VMEM((count, GROUP), bf16),
            pltpu.VMEM((count, GROUP), bf16),
            pltpu.VMEM((count, GROUP), f32),
            pltpu.VMEM((nchunk, GROUP, GROUP), bf16),
            pltpu.VMEM((nchunk, HALO, GROUP), f32),
            pltpu.VMEM((count, GROUP), bf16),
            pltpu.VMEM((count, GROUP), f32),
            pltpu.VMEM((count, GROUP), bf16),
            pltpu.VMEM((count, GROUP), f32),
            pltpu.VMEM((count, ncols), f32),
            pltpu.VMEM((1, feats), f32),
            pltpu.VMEM((1, GROUP), f32),
            pltpu.VMEM((1, GROUP), f32),
            pltpu.VMEM((1, GROUP), f32),
            pltpu.VMEM((TAPS, GROUP), bf16),
            pltpu.VMEM((count, GROUP), bf16),
            pltpu.VMEM((count, GROUP), bf16),
            pltpu.VMEM((HALO + count, GROUP), f32),
            pltpu.VMEM((GROUP, GROUP), f32),
            pltpu.VMEM((ny, GROUP + LOGS, GROUP), bf16),
            pltpu.VMEM((nz, GROUP + LOGS, GROUP), bf16),
            pltpu.VMEM((HALO, GROUP), f32),
            pltpu.VMEM((HALO, GROUP), f32),
            sems((nb,)), sems((4,)), sems((6,)), sems((1,)),
            pltpu.SemaphoreType.REGULAR((1,)), pltpu.SemaphoreType.REGULAR((1,)),
            sems((1,)), sems((2,)), sems((1,)), sems((3,)),
            sems((1,)), sems((1,)), sems((nz,)), sems((nz,)), sems((1,)), sems((1,)),
            sems((1,)), sems((2, nb)), sems((2, nb)), sems((2, nb)),
        ],
        compiler_params=pltpu.CompilerParams(
            vmem_limit_bytes=40 * 2**20, collective_id=0, has_side_effects=True
        ),
    )(*[pltpu.with_memory_space_constraint(a, pltpu.HBM) for a in (
        tokens, in_gain[None], w_query, w_forget, w_input, w_outgate, w_conv_h, w_conv_b, w_conv_c,
        forget_floor[None], forget_leak, state_gain[None], conv_taps, group_gain[None],
        out_state, out_conv,
    )])


def solution(mesh):
    cols, rows = P(None, "tp"), P("tp", None)
    in_specs = (
        P("sp", None), P(), cols, cols, cols, cols, cols, cols, cols,
        P("tp"), P("sp", "tp"), P(), cols, P(), rows, rows,
    )
    return jax.shard_map(
        body, mesh=mesh, in_specs=in_specs, out_specs=P("sp", "tp"), check_vma=False
    )
```

time: 39.8 us -> 36.4 us (0.915)
  the two profiles are of different devices: /device:TPU:192 before, /device:TPU:1 now
where the time goes in v3:
time: 36.4 us; the launch traced here: 36.3 us
  Pallas kernels  35.5 us (98%)
  local copies, waits for them, and re-layouts  0.8 us (2%)
    pallas_call x1, Pallas kernels, body(): pl.pallas_call(functools.partial(fused_kernel, tp, ny, nz), in_specs=[hbm...  35.5 us
    unnamed x1, local copies, waits for them, and re-layouts  0.8 us

profile of v3, /device:TPU:1, one launch (start us, length us, event | category | flops | bytes accessed | tf_op | source)
XLA Modules:
  0.0 36.3 jit_solution(14332190054807660293)
XLA Ops:
  0.0 35.5 %shard_map.154 = bf16[1024,256]{1,0:T(8,128)(2,1)S(1)} custom-call(bf16[1024,2048]{1,0:T(8,128)(2,1)} %tokens.1, f32[1,2048]{1,0:T(1,128)} %bitcast.4, bf16[2048,128]{1,0:T(8,128)(2,1)} %wq.1, bf16[2048,128]{1,0:T(8,128)(2,1)} %wf.1, bf16[2048,128]{1,0:T(8,128)(2,1)} %wi.1, bf16[2048,128]{1,0:T(8,128)(2,1)} %wg.1, bf16[2048,128]{1,0:T(8,128)(2,1)} %wh.1, ...), custom_call_target="tpu_custom_call" | custom-call | tf_op jit(solution)/shard_map/pallas_call | solution.py:604
  35.5 0.8 %copy.18 = bf16[1024,256]{1,0:T(8,128)(2,1)} copy(bf16[1024,256]{1,0:T(8,128)(2,1)S(1)} %shard_map.154) | data formatting | bytes 1048576

commit v4 on v3

--- a/solution.py
+++ b/solution.py
@@ -42,7 +42,7 @@
     tokens, in_gain, wq, wf, wi, wg, wh, wb, wc, floor, leak, state_gain, taps, group_gain,
     out_state, out_conv, result,
     tok, w, leakv, cols, mixed, xs, kmid, val, emid, old, stats, gate, read, qdev, scl, acc,
-    gainv, floorv, sgainv, ggainv, tapsv, prods, wide,
+    gainv, floorv, sgainv, ggainv, tapsv, prods, wide, keyv, terms, kend,
     pad, incoming, ybuf, zbuf, rim, tail,
     tok_sem, w_sem, small_sem, own_sem, ready_z, ready_rim,
     colx_send, colx_recv, coly_send, coly_recv,
@@ -221,6 +221,10 @@
     def _():
         pl.semaphore_signal(barrier, inc=1, device_id={"sp": place + 1})
 
+    for t in range(1, nb):
+        tok_copy(t).start()
+    smalls[2].start()
+
     def meet():
         with scope("barrier"):
             across = jnp.where(yy == 0, jnp.minimum(zz, 1), 0)
@@ -273,33 +277,40 @@
         xs[here, :] = (both[:, :GROUP] * scale).astype(bf16)
         val[here, :] = (both[:, GROUP:] * scale).astype(bf16)
 
-    def chain(t, carry):
-        state, offset = carry
+    def logs(t):
         here = span(t)
         key = (1.0 - floorv[...]) * jax.nn.sigmoid(-xs[here, :].astype(f32))
-        terms = split(jnp.log(1.0 - key) + leakv[here, :])
-        cums = []
-        for b in range(per):
-            rows = slice(b * CHUNK, (b + 1) * CHUNK)
-            sums = dot(ones, jnp.concatenate([term[rows] for term in terms], axis=1))
-            cums.append(sums[:, :GROUP] + sums[:, GROUP:])
-        fresh = []
-        for b in range(per):
-            chunk, cum = t * per + b, cums[b]
-            at = slice(chunk * CHUNK, (chunk + 1) * CHUNK)
-            mid = cum[CHUNK // 2 - 1 : CHUNK // 2]
-            last = cum[CHUNK - 1 : CHUNK]
-            emid[at, :] = jnp.exp(cum - mid)
-            k_mid = key[b * CHUNK : (b + 1) * CHUNK] * jnp.exp(mid - cum)
-            kmid[at, :] = k_mid.astype(bf16)
-            k_end = (k_mid * jnp.exp(last - mid)).astype(bf16)
-            stats[chunk, 0:1] = mid
-            fresh.append(dot(val[at, :], k_end, ((0,), (0,))))
-        for b in range(per):
-            chunk, last = t * per + b, cums[b][CHUNK - 1 : CHUNK]
+        keyv[here, :] = key
+        hi, low = split(jnp.log(1.0 - key) + leakv[here, :])
+        terms[here, :GROUP] = hi
+        terms[here, GROUP:] = low
+
+    def piece(chunk):
+        return slice(chunk * CHUNK, (chunk + 1) * CHUNK)
+
+    def sums(chunk):
+        both = dot(ones, terms[piece(chunk), :])
+        emid[piece(chunk), :] = both[:, :GROUP] + both[:, GROUP:]
+
+    def decays(chunk):
+        at = piece(chunk)
+        cum = emid[at, :]
+        mid = cum[CHUNK // 2 - 1 : CHUNK // 2]
+        last = cum[CHUNK - 1 : CHUNK]
+        stats[chunk, 0:1] = mid
+        stats[chunk, 2:3] = last
+        emid[at, :] = jnp.exp(cum - mid)
+        k_mid = keyv[at, :] * jnp.exp(mid - cum)
+        kmid[at, :] = k_mid.astype(bf16)
+        kend[at, :] = (k_mid * jnp.exp(last - mid)).astype(bf16)
+
+    def own_state():
+        state, offset = jnp.zeros((GROUP, GROUP), f32), jnp.zeros((1, GROUP), f32)
+        for chunk in range(nchunk):
+            at, last = piece(chunk), stats[chunk, 2:3]
             old[chunk] = state.astype(bf16)
             stats[chunk, 1:2] = offset
-            state = state * jnp.exp(last) + fresh[b]
+            state = state * jnp.exp(last) + dot(val[at, :], kend[at, :], ((0,), (0,)))
             offset = offset + last
         return state, offset
 
@@ -308,13 +319,9 @@
         right = (both[:, GROUP:] * factor).astype(bf16).astype(f32)
         return (left * right).astype(bf16).astype(f32)
 
-    carry = (jnp.zeros((GROUP, GROUP), f32), jnp.zeros((1, GROUP), f32))
     with scope("load0"):
         smalls[0].wait()
         tok_copy(0).wait()
-    smalls[2].start()
-    for t in range(1, nb):
-        tok_copy(t).start()
     for i in range(2, 7):
         w_copy(i).start()
     for copy in smalls[3:]:
@@ -324,34 +331,14 @@
     with scope("load1"):
         w_wait(0, 2)
         smalls[1].wait()
-    with scope("A"):
-        project_states(0)
-        smalls[2].wait()
-        for t in range(1, nb):
-            with scope("tokwait"):
-                tok_copy(t).wait()
+    for t in range(1, nb):
+        with scope("tokwait"):
+            tok_copy(t).wait()
+        with scope("A"):
             prepare(t)
-            carry = chain(t - 1, carry)
-            project_states(t)
-            if t == 1:
-                meet()
-
-    with scope("w23wait"):
-        w_wait(2, 4)
-    with scope("rimsend"):
-        end = slice(count - 2 * HALO, count)
-        tail[...] = gated_inputs(dot(tok[end, :], w[:, lanes(2, 4)]), scl[end, :])[HALO:]
-
-        @pl.when(jnp.logical_and(yy == ny - 1, zz < nz - 1))
-        def _():
-            pl.semaphore_wait(ready_rim.at[0], 1)
-
-        @pl.when(place < sp - 1)
-        def _():
-            rim_copy.start()
-
-    with scope("A2"):
-        carry = chain(nb - 1, carry)
+            project_states(t - 1)
+        if t == 2:
+            meet()
 
     def pack(slot, matrix, logs):
         hi = logs.astype(bf16)
@@ -365,19 +352,10 @@
         logs = slot[GROUP : GROUP + LOGS, :].astype(f32)
         return slot[0:GROUP, :].astype(f32), logs[0:1] + logs[1:2] + logs[2:3]
 
-    pack(ybuf.at[yy], *carry)
-    for r in range(1, ny):
-        y_copy(r).start()
-
-    with scope("w46wait"):
-        w_wait(4, 6)
-        w_wait(6, 7)
-        for copy in smalls[3:]:
-            copy.wait()
-    taps_f = tapsv[...].astype(f32)
     pad[0:HALO, :] = jnp.zeros((HALO, GROUP), f32)
 
     def convolve(first, size, conv_in, proj_b):
+        taps_f = tapsv[...].astype(f32)
         total = taps_f[TAPS - 1 : TAPS] * conv_in
         for j in range(TAPS - 1):
             start = HALO - (TAPS - 1) + j + first
@@ -462,31 +440,62 @@
             shared_in(0).wait_recv()
         share_all(y_behind, y_ahead, 2)
 
-    with scope("B"):
+    with scope("w23wait"):
+        w_wait(2, 4)
+        smalls[2].wait()
+    with scope("A2"):
+        project_states(nb - 1)
+        logs(0)
+        logs(1)
+        project_inputs(nb - 1)
+        logs(2)
+        logs(3)
+        tail[...] = pad[count : count + HALO, :]
         project_inputs(0)
+        for chunk in range(nchunk):
+            sums(chunk)
+        for chunk in range(nchunk):
+            decays(chunk)
         project_inputs(1)
+        pack(ybuf.at[yy], *own_state())
+    with scope("rimsend"):
+        @pl.when(jnp.logical_and(yy == ny - 1, zz < nz - 1))
+        def _():
+            pl.semaphore_wait(ready_rim.at[0], 1)
+
+        @pl.when(place < sp - 1)
+        def _():
+            rim_copy.start()
+
+        for r in range(1, ny):
+            y_copy(r).start()
+
+    with scope("w46wait"):
+        w_wait(4, 6)
+        w_wait(6, 7)
+        for copy in smalls[3:]:
+            copy.wait()
+    with scope("B1"):
         project_gates(1)
         conv(1)
+        project_gates(0)
         send(1, 1)
-        project_gates(0)
-        first_rows()
-    share()
-    combine()
     with scope("B2"):
         project_inputs(2)
         project_gates(2)
         conv(2)
         project_query(0)
         send(1, 2)
+    first_rows()
     with scope("B3"):
-        project_inputs(3)
         project_gates(3)
         conv(3)
-        project_query(1)
         reads(0)
         reads(1)
         send(1, 3)
+    combine()
     with scope("C2"):
+        project_query(1)
         project_query(2)
         reads(2)
         reads(3)
@@ -496,9 +505,9 @@
     with scope("C3"):
         reads(6)
         reads(7)
-
-    share_on()
-    conv_order = [1, 0] + list(range(2, nb))
+    share()
+
+    conv_order = [1, 2, 0, 3]
     with scope("relayconv"):
         for t in conv_order[:-1]:
             relay_first(1, t)
@@ -540,6 +549,7 @@
 
     with scope("relayconvlast"):
         relay_first(1, conv_order[-1])
+    share_on()
     for t in range(nb - 1):
         with scope("relaystate"):
             relay_first(0, t)
@@ -630,6 +640,9 @@
             pltpu.VMEM((TAPS, GROUP), bf16),
             pltpu.VMEM((count, GROUP), bf16),
             pltpu.VMEM((count, GROUP), bf16),
+            pltpu.VMEM((count, GROUP), f32),
+            pltpu.VMEM((count, 2 * GROUP), bf16),
+            pltpu.VMEM((count, GROUP), bf16),
             pltpu.VMEM((HALO + count, GROUP), f32),
             pltpu.VMEM((GROUP, GROUP), f32),
             pltpu.VMEM((ny, GROUP + LOGS, GROUP), bf16),

time: 36.4 us -> 34.7 us (0.953); the launches traced: 36.3 us -> 34.2 us
  Pallas kernels: 35.5 us -> 33.4 us
    pallas_call x1, Pallas kernels: 35.5 us -> 33.4 us  [body(): pl.pallas_call(functools.partial(fused_kernel, tp, ny, nz), in_specs=[hbm...]
where the time goes in v4:
time: 34.7 us; the launch traced here: 34.2 us
  Pallas kernels  33.4 us (96%)
  local copies, waits for them, and re-layouts  0.8 us (2%)
    pallas_call x1, Pallas kernels, body(): pl.pallas_call(functools.partial(fused_kernel, tp, ny, nz), in_specs=[hbm...  33.4 us
    unnamed x1, local copies, waits for them, and re-layouts  0.8 us

profile of v4, /device:TPU:1, one launch (start us, length us, event | category | flops | bytes accessed | tf_op | source)
XLA Modules:
  0.0 34.2 jit_solution(11344268492873734034)
XLA Ops:
  0.0 33.4 %shard_map.154 = bf16[1024,256]{1,0:T(8,128)(2,1)S(1)} custom-call(bf16[1024,2048]{1,0:T(8,128)(2,1)} %tokens.1, f32[1,2048]{1,0:T(1,128)} %bitcast.4, bf16[2048,128]{1,0:T(8,128)(2,1)} %wq.1, bf16[2048,128]{1,0:T(8,128)(2,1)} %wf.1, bf16[2048,128]{1,0:T(8,128)(2,1)} %wi.1, bf16[2048,128]{1,0:T(8,128)(2,1)} %wg.1, bf16[2048,128]{1,0:T(8,128)(2,1)} %wh.1, ...), custom_call_target="tpu_custom_call" | custom-call | tf_op jit(solution)/shard_map/pallas_call | solution.py:614
  33.4 0.8 %copy.18 = bf16[1024,256]{1,0:T(8,128)(2,1)} copy(bf16[1024,256]{1,0:T(8,128)(2,1)S(1)} %shard_map.154) | data formatting | bytes 1048576

commit v5 on v4

--- a/solution.py
+++ b/solution.py
@@ -335,8 +335,8 @@
         with scope("tokwait"):
             tok_copy(t).wait()
         with scope("A"):
+            project_states(t - 1)
             prepare(t)
-            project_states(t - 1)
         if t == 2:
             meet()
 
@@ -413,11 +413,11 @@
             def _():
                 pl.semaphore_wait(ready_z.at[0], nz - 1 - zz)
 
-        def send_z(target, _):
-            z_copy(target).start()
+        def send_z(step, _):
+            z_copy(nz - 1 - step).start()
             return 0
 
-        lax.fori_loop(zz + 1, nz, send_z, 0)
+        lax.fori_loop(0, nz - 1 - zz, send_z, 0)
 
     def first_rows():
         with scope("rimwait"):
@@ -494,6 +494,7 @@
         reads(1)
         send(1, 3)
     combine()
+    share()
     with scope("C2"):
         project_query(1)
         project_query(2)
@@ -505,11 +506,10 @@
     with scope("C3"):
         reads(6)
         reads(7)
-    share()
 
     conv_order = [1, 2, 0, 3]
     with scope("relayconv"):
-        for t in conv_order[:-1]:
+        for t in conv_order:
             relay_first(1, t)
 
     incoming[...] = jnp.zeros_like(incoming)
@@ -547,23 +547,21 @@
             side = cols[tp : 2 * tp].reshape(tp * GROUP, ncols)
             acc[span(t), :] = dot(mixed[t, :, tp * GROUP :], side)
 
-    with scope("relayconvlast"):
-        relay_first(1, conv_order[-1])
     share_on()
-    for t in range(nb - 1):
+    with scope("relayconv2"):
+        for t in conv_order[:-1]:
+            relay_second(1, t)
+    for t in range(nb):
         with scope("relaystate"):
             relay_first(0, t)
-        with scope("relayconv2"):
-            relay_second(1, conv_order[t])
-    with scope("colwait"):
-        own_cols_done.wait()
-        partner_cols_in.wait_recv()
-        shared_in(1).wait_recv()
-        shared_in(2).wait_recv()
-    for t in conv_order[:-1]:
-        conv_dot(t)
-    with scope("relaystate"):
-        relay_first(0, nb - 1)
+        if t == 1:
+            with scope("colwait"):
+                own_cols_done.wait()
+                partner_cols_in.wait_recv()
+                shared_in(1).wait_recv()
+                shared_in(2).wait_recv()
+        if t > 0:
+            conv_dot(conv_order[t - 1])
     with scope("relayconv2last"):
         relay_second(1, conv_order[-1])
 
@@ -577,10 +575,9 @@
     for t in range(nb):
         with scope("finfar"):
             relay_second(0, t)
-        if t == 0:
-            conv_dot(conv_order[-1])
-        else:
+        if t > 0:
             finish(t - 1)
+    conv_dot(conv_order[-1])
     finish(nb - 1)
 
     with scope("drain"):

time: 34.7 us -> 33.2 us (0.957)
  Pallas kernels: 33.4 us -> 32.2 us
    pallas_call x1, Pallas kernels: 33.4 us -> 32.2 us  [body(): pl.pallas_call(functools.partial(fused_kernel, tp, ny, nz), in_specs=[hbm...]
where the time goes in v5:
time: 33.2 us; the launch traced here: 33 us
  Pallas kernels  32.2 us (97%)
  local copies, waits for them, and re-layouts  0.8 us (2%)
    pallas_call x1, Pallas kernels, body(): pl.pallas_call(functools.partial(fused_kernel, tp, ny, nz), in_specs=[hbm...  32.2 us
    unnamed x1, local copies, waits for them, and re-layouts  0.8 us

profile of v5, /device:TPU:1, one launch (start us, length us, event | category | flops | bytes accessed | tf_op | source)
XLA Modules:
  0.0 33.0 jit_solution(502732614910363672)
XLA Ops:
  0.0 32.2 %shard_map.154 = bf16[1024,256]{1,0:T(8,128)(2,1)S(1)} custom-call(bf16[1024,2048]{1,0:T(8,128)(2,1)} %tokens.1, f32[1,2048]{1,0:T(1,128)} %bitcast.4, bf16[2048,128]{1,0:T(8,128)(2,1)} %wq.1, bf16[2048,128]{1,0:T(8,128)(2,1)} %wf.1, bf16[2048,128]{1,0:T(8,128)(2,1)} %wi.1, bf16[2048,128]{1,0:T(8,128)(2,1)} %wg.1, bf16[2048,128]{1,0:T(8,128)(2,1)} %wh.1, ...), custom_call_target="tpu_custom_call" | custom-call | tf_op jit(solution)/shard_map/pallas_call | solution.py:611
  32.2 0.8 %copy.18 = bf16[1024,256]{1,0:T(8,128)(2,1)} copy(bf16[1024,256]{1,0:T(8,128)(2,1)S(1)} %shard_map.154) | data formatting | bytes 1048576

commit v6 on v5

--- a/solution.py
+++ b/solution.py
@@ -535,11 +535,14 @@
         total = read[here, :] + dot(qdev[here, :], incoming[...].astype(bf16), ((1,), (1,)))
         out = rms(total) * sgainv[...] * jax.nn.silu(gate[here, :].astype(f32))
         put(0, t, out.astype(bf16))
-        send(0, t)
 
     with scope("merge"):
-        for t in range(nb):
+        merge(0)
+        send(0, 0)
+        for t in range(1, nb):
             merge(t)
+        for t in range(1, nb):
+            send(0, t)
 
     def conv_dot(t):
         with scope("convdot"):
@@ -551,25 +554,31 @@
     with scope("relayconv2"):
         for t in conv_order[:-1]:
             relay_second(1, t)
-    for t in range(nb):
+    with scope("relaystate"):
+        relay_first(0, 0)
+    with scope("relayconv2last"):
+        relay_second(1, conv_order[-1])
+    with scope("colwait"):
+        own_cols_done.wait()
+        partner_cols_in.wait_recv()
+        shared_in(1).wait_recv()
+        shared_in(2).wait_recv()
+    conv_dot(conv_order[0])
+    conv_dot(conv_order[1])
+    with scope("relaystate"):
+        relay_first(0, 1)
+    conv_dot(conv_order[2])
+    for t in range(2, nb):
         with scope("relaystate"):
             relay_first(0, t)
-        if t == 1:
-            with scope("colwait"):
-                own_cols_done.wait()
-                partner_cols_in.wait_recv()
-                shared_in(1).wait_recv()
-                shared_in(2).wait_recv()
-        if t > 0:
-            conv_dot(conv_order[t - 1])
-    with scope("relayconv2last"):
-        relay_second(1, conv_order[-1])
+    conv_dot(conv_order[3])
 
     def finish(t):
         with scope("finwait"):
             pair_wait(0, t)
         with scope("findot"):
-            total = acc[span(t), :] + dot(mixed[t, :, : tp * GROUP], cols[0:tp].reshape(tp * GROUP, ncols))
+            main = cols[0:tp].reshape(tp * GROUP, ncols)
+            total = acc[span(t), :] + dot(mixed[t, :, : tp * GROUP], main)
             result[span(t), :] = total.astype(bf16)
 
     for t in range(nb):
@@ -577,7 +586,6 @@
             relay_second(0, t)
         if t > 0:
             finish(t - 1)
-    conv_dot(conv_order[-1])
     finish(nb - 1)
 
     with scope("drain"):

time: 33.2 us -> 33.8 us (1.018)
  Pallas kernels: 32.2 us -> 32.9 us
    pallas_call x1, Pallas kernels: 32.2 us -> 32.9 us  [body(): pl.pallas_call(functools.partial(fused_kernel, tp, ny, nz), in_specs=[hbm...]
where the time goes in v6:
time: 33.8 us; the launch traced here: 33.7 us
  Pallas kernels  32.9 us (97%)
  local copies, waits for them, and re-layouts  0.8 us (2%)
    pallas_call x1, Pallas kernels, body(): pl.pallas_call(functools.partial(fused_kernel, tp, ny, nz), in_specs=[hbm...  32.9 us
    unnamed x1, local copies, waits for them, and re-layouts  0.8 us

profile of v6, /device:TPU:1, one launch (start us, length us, event | category | flops | bytes accessed | tf_op | source)
XLA Modules:
  0.0 33.7 jit_solution(10028717952427550835)
XLA Ops:
  0.0 32.9 %shard_map.154 = bf16[1024,256]{1,0:T(8,128)(2,1)S(1)} custom-call(bf16[1024,2048]{1,0:T(8,128)(2,1)} %tokens.1, f32[1,2048]{1,0:T(1,128)} %bitcast.4, bf16[2048,128]{1,0:T(8,128)(2,1)} %wq.1, bf16[2048,128]{1,0:T(8,128)(2,1)} %wf.1, bf16[2048,128]{1,0:T(8,128)(2,1)} %wi.1, bf16[2048,128]{1,0:T(8,128)(2,1)} %wg.1, bf16[2048,128]{1,0:T(8,128)(2,1)} %wh.1, ...), custom_call_target="tpu_custom_call" | custom-call | tf_op jit(solution)/shard_map/pallas_call | solution.py:619
  32.9 0.8 %copy.18 = bf16[1024,256]{1,0:T(8,128)(2,1)} copy(bf16[1024,256]{1,0:T(8,128)(2,1)S(1)} %shard_map.154) | data formatting | bytes 1048576
